TPU v7x, 256 devices: a whole 4x4x8 slice. The times are simulated.
256 devices in a mesh: sp: 32 (over z, y), tp: 8 (over x, core).
Axes of the slice: x: 4, y: 4, z: 8, core: 2. Of those that a mesh axis runs over, the one named last changes fastest.
Arguments:
- tokens: bfloat16 [16384, 2048], P(('sp', 'tp')), may hold values from -8 to 8, as said below
- w_query: bfloat16 [2048, 1024], P(None, 'tp'), may hold values from -0.125 to 0.125
- w_key: bfloat16 [2048, 1024], P(None, 'tp'), may hold values from -0.125 to 0.125
- w_value: bfloat16 [2048, 1024], P(None, 'tp'), may hold values from -0.125 to 0.125
- head_bias: float32 [16], P('tp'), may hold values from -40 to -3
- w_out: bfloat16 [1024, 2048], P('tp'), may hold values from -0.1875 to 0.1875
Outputs:
- mixed: bfloat16 [16384, 2048], P(('sp', 'tp'))
Inputs may be any that keep to these rules, and one draw needn't show every extreme that they name: `tokens`: activations of order one whose mean shifts between blocks of 512 positions.
All inputs are finite; a program needn't handle non-finite values.
Results may differ from a plain program's by a relative error of at most 0.014.
Values may be sent and summed in bfloat16 or wider, within the bound.
A program may use at most 128 MiB of HBM per device.

v0:
```python
import functools
import math

import jax
import jax.numpy as jnp
from jax import lax
from jax.experimental import pallas as pl
from jax.experimental.pallas import tpu as pltpu
from jax.sharding import PartitionSpec as P

MESH = pl.DeviceIdType.MESH
LOG2E = math.log2(math.e)
CHUNK = 256
PARTS = 4
COLS = 512
LOOK = 4
LOG_MAX = 126.0


def layer_kernel(
    n_sp, n_tp, heads, bias_ref, tokens_ref, wq_ref, wk_ref, wv_ref, wo_ref, out_ref,
    tok, wqkv, wfull, kv_own, q_own, q_all, kv_all, packed, att, att_rows, tri,
    load_sem, tok_send, tok_recv, wo_send, wo_recv, kv_send, pass_send, kv_recv, q_send, q_recv,
    back_send, back_recv,
):
    me = lax.axis_index("sp")
    col = lax.axis_index("tp")
    share_count = n_sp // heads
    device_rows = PARTS * tokens_ref.shape[1]
    rows, width = kv_own.shape[2], kv_own.shape[3]
    half = width // 2
    piece = min(rows, device_rows)
    pieces = rows // piece
    subs = device_rows // piece
    chunk_shares = CHUNK // rows
    seg_chunks = share_count * rows // CHUNK
    my_head = me // share_count
    my_share = lax.rem(me, share_count)
    core = lax.rem(col, 2)
    place = col // 2
    places = n_tp // 2
    sibling = place * 2 + 1 - core

    loads = [
        pltpu.make_async_copy(src, dst, load_sem.at[index])
        for index, (src, dst) in enumerate(
            [
                (tokens_ref, tok.at[col]),
                (wq_ref, wqkv.at[0]),
                (wk_ref, wqkv.at[1]),
                (wv_ref, wqkv.at[2]),
                (wo_ref, wfull.at[col]),
            ]
        )
    ]
    for copy in loads:
        copy.start()

    barrier = pltpu.get_barrier_semaphore()
    total = n_sp * n_tp
    flat = me * n_tp + col

    def greet(step, carry):
        other = lax.rem(flat + step, total)
        pl.semaphore_signal(
            barrier, inc=1, device_id=(other // n_tp, lax.rem(other, n_tp)), device_id_type=MESH
        )
        return carry

    lax.fori_loop(1, total, greet, 0)
    key_id = lax.broadcasted_iota(jnp.int32, (CHUNK, CHUNK), 0)
    out_id = lax.broadcasted_iota(jnp.int32, (CHUNK, CHUNK), 1)
    tri[...] = jnp.where(key_id > out_id, 1.0, 0.0).astype(jnp.bfloat16)
    pl.semaphore_wait(barrier, total - 1)

    def same_core(k):
        return lax.rem(place + k, places) * 2 + core

    def arrived(ref, sem):
        pltpu.make_async_copy(ref, ref, sem).wait()

    def token_copy(kind, part):
        if kind < places:
            src, block = tokens_ref.at[part], col
            target = sibling if kind == 0 else same_core(kind)
        else:
            block = same_core(kind - places + 1)
            src, target = tok.at[block, part], sibling
        return pltpu.make_async_remote_copy(
            src_ref=src, dst_ref=tok.at[block, part],
            send_sem=tok_send.at[kind, part], recv_sem=tok_recv.at[block, part],
            device_id=(me, target), device_id_type=MESH,
        )

    def wo_copy(kind):
        if kind < places:
            src, block = wo_ref, col
            target = sibling if kind == 0 else same_core(kind)
        else:
            block = same_core(kind - places + 1)
            src, target = wfull.at[block], sibling
        return pltpu.make_async_remote_copy(
            src_ref=src, dst_ref=wfull.at[block],
            send_sem=wo_send.at[kind], recv_sem=wo_recv.at[block],
            device_id=(me, target), device_id_type=MESH,
        )

    for part in range(PARTS):
        for kind in range(places):
            token_copy(kind, part).start()

    lane = lax.broadcasted_iota(jnp.int32, (rows, width), 1)
    lane_half = lax.broadcasted_iota(jnp.int32, (rows // 2, width), 1)

    def turn(value):
        return pltpu.roll(value, half, 1)

    def kv_copy(step, share):
        head = lax.rem(my_head + step, heads)
        return pltpu.make_async_remote_copy(
            src_ref=kv_own.at[head, share], dst_ref=kv_all.at[me, share],
            send_sem=kv_send.at[step, share], recv_sem=kv_recv.at[me, share],
            device_id=(head * share_count + my_share, col), device_id_type=MESH,
        )

    def forward(turn_of, step, share):
        block = turn_of * share_count + my_share
        peer = my_head * share_count + lax.rem(my_share + step, share_count)
        return pltpu.make_async_remote_copy(
            src_ref=kv_all.at[block, share], dst_ref=kv_all.at[block, share],
            send_sem=pass_send.at[turn_of, step, share], recv_sem=kv_recv.at[block, share],
            device_id=(peer, col), device_id_type=MESH,
        )

    def relay(block):
        for share in range(share_count):
            arrived(kv_all.at[block, share], kv_recv.at[block, share])
            for step in range(1, share_count):
                forward(block // share_count, step, share).start()

    def share_of(peer):
        return lax.rem(lax.rem(peer, share_count) + me, share_count)

    def q_copy(step):
        peer = lax.rem(me + step, n_sp)
        return pltpu.make_async_remote_copy(
            src_ref=q_own.at[peer // share_count, share_of(peer)], dst_ref=q_all.at[me],
            send_sem=q_send.at[step], recv_sem=q_recv.at[me],
            device_id=(peer, col), device_id_type=MESH,
        )

    def project(group):
        x = tok[pl.ds(group * pieces, pieces)].reshape(subs * rows, tok.shape[3])
        qf = jnp.dot(x, wqkv[0], preferred_element_type=jnp.float32) * (LOG2E * half ** (-0.5))
        kf = jnp.dot(x, wqkv[1], preferred_element_type=jnp.float32)
        vf = jnp.dot(x, wqkv[2], preferred_element_type=jnp.float32)
        for sub in range(subs):
            own = slice(sub * rows, (sub + 1) * rows)
            publish(group * subs + sub, qf[own], kf[own], vf[own])

    def publish(share, qf, kf, vf):
        for pair in range(heads // 2):
            cols = slice(pair * width, (pair + 1) * width)
            kk, vv = kf[:, cols], vf[:, cols]
            top, low = qf[: rows // 2, cols], qf[rows // 2 :, cols]
            kv_own[2 * pair, share] = jnp.where(lane < half, kk, turn(vv)).astype(jnp.bfloat16)
            kv_own[2 * pair + 1, share] = jnp.where(lane < half, turn(kk), vv).astype(jnp.bfloat16)
            q_own[2 * pair, share] = jnp.where(lane_half < half, top, turn(low)).astype(
                jnp.bfloat16
            )
            q_own[2 * pair + 1, share] = jnp.where(lane_half < half, turn(top), low).astype(
                jnp.bfloat16
            )
        for step in range(1, heads):
            kv_copy(step, share).start()
        kv_all[me, share] = kv_own[my_head, share]
        for step in range(1, share_count):
            forward(my_head, step, share).start()
        for step in range(1, n_sp):

            @pl.when(share_of(lax.rem(me + step, n_sp)) == share)
            def _():
                q_copy(step).start()

        @pl.when(share_of(me) == share)
        def _():
            q_all[me] = q_own[my_head, share]

    for copy in loads:
        copy.wait()
    own_group = col // pieces
    groups = n_tp // pieces
    if pieces > 1:
        for part in range(PARTS):
            arrived(tok.at[sibling, part], tok_recv.at[sibling, part])
        project(own_group)
    for part in range(PARTS):
        for k in range(1, places):
            block = same_core(k)
            arrived(tok.at[block, part], tok_recv.at[block, part])
            token_copy(places + k - 1, part).start()
    for kind in range(places):
        wo_copy(kind).start()
    for part in range(PARTS):
        if pieces == 1:
            arrived(tok.at[sibling, part], tok_recv.at[sibling, part])
        for k in range(1, places):
            block = lax.rem(place + k, places) * 2 + 1 - core
            arrived(tok.at[block, part], tok_recv.at[block, part])

    def project_next(step, carry):
        project(lax.rem(own_group + step, groups))
        return carry

    lax.fori_loop(1 if pieces > 1 else 0, groups, project_next, 0)

    bias = bias_ref[my_head] * LOG2E

    def logs(q, keys):
        scores = lax.dot_general(
            q, keys, (((1,), (1,)), ((), ())), preferred_element_type=jnp.float32
        )
        z = scores + bias
        lose = jnp.maximum(
            jnp.log(1.0 + jnp.exp2(jnp.minimum(z, LOG_MAX))) * LOG2E, z
        )
        return z - lose, lose

    def tails(lose):
        lose = lose.astype(jnp.bfloat16)
        tail = jnp.dot(lose, tri[...], preferred_element_type=jnp.float32)
        return tail, tail[:, 0:1] + lose[:, 0:1].astype(jnp.float32)

    def chunk_keys(index):
        block, inner = index // seg_chunks, lax.rem(index, seg_chunks)
        return kv_all[block, pl.ds(inner * chunk_shares, chunk_shares)].reshape(CHUNK, width)

    def weigh(log_take, tail, later, keys):
        weight = jnp.exp2(log_take - tail).astype(jnp.bfloat16)
        return jnp.exp2(-later) * jnp.dot(weight, keys, preferred_element_type=jnp.float32)

    def landing(first_row):
        return (col * heads + my_head) * subs + lax.rem(first_row // piece, subs)

    def is_here(block, index, first_row):
        return jnp.logical_and(block == me, (first_row + index * piece) // device_rows == col)

    def back(block, index, first_row):
        owner = (first_row + index * piece) // device_rows
        slot = landing(first_row)
        return pltpu.make_async_remote_copy(
            src_ref=packed.at[block, index], dst_ref=att.at[slot],
            send_sem=back_send.at[block, index], recv_sem=back_recv.at[slot],
            device_id=(block, owner), device_id_type=MESH,
        )

    def relayed(block):
        return jnp.logical_and(lax.rem(block, share_count) == my_share, block != me)

    for block in range(LOOK):

        @pl.when(relayed(block))
        def _():
            relay(block)

    def visit(block, carry):
        ahead = block + LOOK

        @pl.when(jnp.logical_and(ahead < n_sp, relayed(ahead)))
        def _():
            relay(ahead)

        @pl.when(lax.rem(block, share_count) != my_share)
        def _():
            for share in range(share_count):
                arrived(kv_all.at[block, share], kv_recv.at[block, share])

        @pl.when(block != me)
        def _():
            arrived(q_all.at[block], q_recv.at[block])

        @pl.when(block == n_sp - 2)
        def _():
            for k in range(1, places):
                arrived(wfull.at[same_core(k)], wo_recv.at[same_core(k)])
                wo_copy(places + k - 1).start()

        pair = q_all[block].astype(jnp.float32)
        low = jnp.where(lane_half < half, pair, 0.0)
        high = jnp.where(lane_half < half, turn(pair), 0.0)
        q = jnp.concatenate([low, high], axis=0).astype(jnp.bfloat16)
        first_row = lax.rem(my_share + block, share_count) * rows
        diagonal = first_row // CHUNK
        q_pos = first_row + lax.broadcasted_iota(jnp.int32, (rows, CHUNK), 0)
        k_pos = diagonal * CHUNK + lax.broadcasted_iota(jnp.int32, (rows, CHUNK), 1)
        live = k_pos < q_pos

        keys = chunk_keys(block * seg_chunks + diagonal)
        log_take, keep = logs(q, keys)
        tail, later = tails(jnp.where(live, keep, 0.0))
        weight = jnp.where(live, jnp.exp2(log_take - tail), 0.0).astype(jnp.bfloat16)
        acc = jnp.dot(weight, keys, preferred_element_type=jnp.float32)

        def single(step, state):
            acc, later = state
            keys = chunk_keys(block * seg_chunks + diagonal - 1 - step)
            log_take, keep = logs(q, keys)
            tail, whole = tails(keep)
            return acc + weigh(log_take, tail, later, keys), later + whole

        def segment(step, state):
            acc, later = state
            first = (block - 1 - step) * seg_chunks
            keys = [chunk_keys(first + index) for index in reversed(range(seg_chunks))]
            terms = [logs(q, part) for part in keys]
            ends = [tails(keep) for _, keep in terms]
            for part, (log_take, _), (tail, whole) in zip(keys, terms, ends):
                acc = acc + weigh(log_take, tail, later, part)
                later = later + whole
            return acc, later

        state = lax.fori_loop(0, diagonal, single, (acc, later))
        acc, _ = lax.fori_loop(0, block, segment, state)
        for index in range(pieces):
            top = acc[index * piece : index * piece + piece // 2]
            low = acc[index * piece + piece // 2 : (index + 1) * piece]
            lanes = lax.broadcasted_iota(jnp.int32, top.shape, 1)
            folded = jnp.where(lanes < half, turn(top), low).astype(jnp.bfloat16)
            packed[block, index] = folded
            here = is_here(block, index, first_row)

            @pl.when(here)
            def _():
                att[landing(first_row)] = folded

            @pl.when(jnp.logical_not(here))
            def _():
                back(block, index, first_row).start()

        return carry

    lax.fori_loop(0, n_sp, visit, 0)

    for sub in range(subs):
        share = (col * device_rows + sub * piece) // rows
        source_share = lax.rem(share + n_sp * share_count - me, share_count)
        for source_col in range(n_tp):
            for pair in range(heads // 2):
                values = []
                for head in (2 * pair, 2 * pair + 1):
                    slot = (source_col * heads + head) * subs + sub
                    source = head * share_count + source_share

                    @pl.when(jnp.logical_not(jnp.logical_and(source == me, source_col == col)))
                    def _():
                        arrived(att.at[slot], back_recv.at[slot])

                    values.append(att[slot].astype(jnp.float32))
                lanes = lax.broadcasted_iota(jnp.int32, values[0].shape, 1)
                top = jnp.where(lanes < half, values[0], turn(values[1]))
                low = jnp.where(lanes < half, turn(values[0]), values[1])
                start = (source_col * heads + 2 * pair) * half
                cols = slice(start, start + width)
                middle = sub * piece + piece // 2
                att_rows[sub * piece : middle, cols] = top.astype(jnp.bfloat16)
                att_rows[middle : (sub + 1) * piece, cols] = low.astype(jnp.bfloat16)

    arrived(wfull.at[sibling], wo_recv.at[sibling])
    for k in range(1, places):
        block = lax.rem(place + k, places) * 2 + 1 - core
        arrived(wfull.at[block], wo_recv.at[block])
    for first in range(0, out_ref.shape[1], COLS):
        w = wfull[:, :, first : first + COLS].reshape(att_rows.shape[1], COLS)
        out_ref[:, first : first + COLS] = jnp.dot(
            att_rows[...], w, preferred_element_type=jnp.float32
        ).astype(jnp.bfloat16)

    for kind in range(2 * places - 1):
        wo_copy(kind).wait_send()
        for part in range(PARTS):
            token_copy(kind, part).wait_send()
    for step in range(1, n_sp):
        q_copy(step).wait_send()
    for share in range(share_count):
        for step in range(1, heads):
            kv_copy(step, share).wait_send()
        for turn_of in range(heads):
            for step in range(1, share_count):
                forward(turn_of, step, share).wait_send()

    def drain(block, carry):
        first_row = lax.rem(my_share + block, share_count) * rows
        for index in range(pieces):
            here = is_here(block, index, first_row)

            @pl.when(jnp.logical_not(here))
            def _():
                back(block, index, first_row).wait_send()

        return carry

    lax.fori_loop(0, n_sp, drain, 0)


def shards(tokens, w_query, w_key, w_value, head_bias, w_out):
    model, local_width = w_query.shape
    heads = head_bias.shape[0]
    width = 2 * (local_width // heads)
    n_sp = lax.axis_size("sp")
    n_tp = lax.axis_size("tp")
    device_rows = tokens.shape[0]
    share_count = n_sp // heads
    rows = device_rows * n_tp // share_count
    piece = min(rows, device_rows)
    pieces = rows // piece
    slots = n_tp * heads * device_rows // piece
    out_width = w_out.shape[1]
    places = n_tp // 2
    kinds = 2 * places - 1

    smem = pl.BlockSpec(memory_space=pltpu.SMEM)
    anywhere = pl.BlockSpec(memory_space=pl.ANY)
    dma = pltpu.SemaphoreType.DMA

    def vmem(*shape):
        return pltpu.VMEM(shape, jnp.bfloat16)

    return pl.pallas_call(
        functools.partial(layer_kernel, n_sp, n_tp, heads),
        out_shape=jax.ShapeDtypeStruct((device_rows, out_width), jnp.bfloat16),
        in_specs=[smem] + [anywhere] * 5,
        out_specs=pl.BlockSpec(memory_space=pltpu.VMEM),
        scratch_shapes=[
            vmem(n_tp, PARTS, device_rows // PARTS, model),
            vmem(3, model, local_width),
            vmem(n_tp, local_width, out_width),
            vmem(heads, share_count, rows, width),
            vmem(heads, share_count, rows // 2, width),
            vmem(n_sp, rows // 2, width),
            vmem(n_sp, share_count, rows, width),
            vmem(n_sp, pieces, piece // 2, width),
            vmem(slots, piece // 2, width),
            vmem(device_rows, n_tp * local_width),
            vmem(CHUNK, CHUNK),
            dma((5,)),
            dma((kinds, PARTS)),
            dma((n_tp, PARTS)),
            dma((kinds,)),
            dma((n_tp,)),
            dma((heads, share_count)),
            dma((heads, share_count, share_count)),
            dma((n_sp, share_count)),
            dma((n_sp,)),
            dma((n_sp,)),
            dma((n_sp, pieces)),
            dma((slots,)),
        ],
        compiler_params=pltpu.CompilerParams(
            collective_id=0, has_side_effects=True, vmem_limit_bytes=60 * 2**20
        ),
        name="layer",
    )(
        head_bias,
        tokens.reshape(PARTS, device_rows // PARTS, model),
        w_query, w_key, w_value, w_out,
    )


def solution(mesh):
    placed = (
        P(("sp", "tp"), None),
        P(None, "tp"),
        P(None, "tp"),
        P(None, "tp"),
        P("tp"),
        P("tp", None),
    )
    return jax.shard_map(
        shards, mesh=mesh, in_specs=placed, out_specs=P(("sp", "tp"), None), check_vma=False
    )
```

profile of v0, /device:TPU:249, one launch (start us, length us, event | category | flops | bytes accessed | tf_op | source)
XLA Modules:
  0.0 407.4 jit_solution(10779227064794238424)
XLA Ops:
  0.0 405.7 %layer.1 = bf16[64,2048]{1,0:T(8,128)(2,1)} custom-call(f32[2]{0:T(128)} %bias_ref.1, bf16[4,16,2048]{2,1,0:T(8,128)(2,1)} %bitcast.1, bf16[2048,128]{1,0:T(8,128)(2,1)} %wq_ref.1, bf16[2048,128]{1,0:T(8,128)(2,1)} %wk_ref.1, bf16[2048,128]{1,0:T(8,128)(2,1)} %wv_ref.1, bf16[128,2048]{1,0:T(8,128)(2,1)} %wo_ref.1), custom_call_target="tpu_custom_call" | custom-call | tf_op jit(solution)/shard_map/layer/pallas_call | solution.py:428
  405.7 1.7 copy.8
where the time goes:
time: 408 us; the launch traced here: 407 us
  Pallas kernels  406 us (100%)
    pallas_call x1, Pallas kernels, shards(): pl.pallas_call(functools.partial(layer_kernel, n_sp, n_tp, heads), out_sh...  406 us

commit v1 on v0

v1 whole, which is shorter than its diff:
```python
import functools
import math

import jax
import jax.numpy as jnp
from jax import lax
from jax.experimental import pallas as pl
from jax.experimental.pallas import tpu as pltpu
from jax.sharding import PartitionSpec as P

MESH = pl.DeviceIdType.MESH
F32, BF16 = jnp.float32, jnp.bfloat16
LOG2E = math.log2(math.e)
PARTS = 4
COLS = 512
EXP_MAX = 126.0
DEAD = -1e30
NZ, NY = 8, 4
SEG = 512
HALF = 256
LANES = 128
DIM = 64
RUN = 64
SHARE = 32
SHARES = SEG // SHARE
TILES = 8
FAR = 1 << 20


def layer_kernel(
    bias_ref, tokens_ref, wq_ref, wk_ref, wv_ref, wo_ref, out_ref,
    tok, wqkv, wfull, proj, bias_all, kv_own, q_own, q_all, kv_all, q_top, q_low, xs, seg_acc,
    seg_keep, packed, att, att_rows,
    load_sem, tok_send, tok_recv, wo_send, wo_recv, bias_send, bias_recv, kv_send, kv_recv,
    ring_send, share_send, q_send, q_recv, back_send, back_recv,
):
    me = lax.axis_index("sp")
    col = lax.axis_index("tp")
    n_sp, n_tp = NZ * NY, 8
    z, y = me // NY, lax.rem(me, NY)
    place, core = col // 2, lax.rem(col, 2)
    places = n_tp // 2
    sibling = place * 2 + 1 - core
    head_core, head_local = y // 2, lax.rem(y, 2)
    mine = core == head_core

    loads = [
        pltpu.make_async_copy(src, dst, load_sem.at[index])
        for index, (src, dst) in enumerate(
            [
                (tokens_ref, tok.at[col]),
                (wq_ref, wqkv.at[:, 0:LANES]),
                (wk_ref, wqkv.at[:, LANES : 2 * LANES]),
                (wv_ref, wqkv.at[:, 2 * LANES : 3 * LANES]),
                (wo_ref, wfull.at[col]),
            ]
        )
    ]
    for copy in loads:
        copy.start()

    barrier = pltpu.get_barrier_semaphore()
    total = n_sp * n_tp
    flat = me * n_tp + col

    def greet(step, carry):
        other = lax.rem(flat + step, total)
        pl.semaphore_signal(
            barrier, inc=1, device_id=(other // n_tp, lax.rem(other, n_tp)), device_id_type=MESH
        )
        return carry

    lax.fori_loop(1, total, greet, 0)
    for head in range(2):
        bias_all[core, head] = jnp.full((8, LANES), bias_ref[head] * LOG2E, F32)
    pl.semaphore_wait(barrier, total - 1)

    def same_core(k):
        return lax.rem(place + k, places) * 2 + core

    def arrived(ref, sem):
        pltpu.make_async_copy(ref, ref, sem).wait()

    def token_copy(kind, part):
        if kind < places:
            src, block = tokens_ref.at[part], col
            target = sibling if kind == 0 else same_core(kind)
        else:
            block = same_core(kind - places + 1)
            src, target = tok.at[block, part], sibling
        return pltpu.make_async_remote_copy(
            src_ref=src, dst_ref=tok.at[block, part],
            send_sem=tok_send.at[kind, part], recv_sem=tok_recv.at[block, part],
            device_id=(me, target), device_id_type=MESH,
        )

    def wo_copy(kind):
        if kind < places:
            src, block = wo_ref, col
            target = sibling if kind == 0 else same_core(kind)
        else:
            block = same_core(kind - places + 1)
            src, target = wfull.at[block], sibling
        return pltpu.make_async_remote_copy(
            src_ref=src, dst_ref=wfull.at[block],
            send_sem=wo_send.at[kind], recv_sem=wo_recv.at[block],
            device_id=(me, target), device_id_type=MESH,
        )

    bias_copy = pltpu.make_async_remote_copy(
        src_ref=bias_all.at[core], dst_ref=bias_all.at[core],
        send_sem=bias_send, recv_sem=bias_recv, device_id=(me, sibling), device_id_type=MESH,
    )

    for part in range(PARTS):
        for kind in range(places):
            token_copy(kind, part).start()
    bias_copy.start()

    def kv_copy(head, half):
        aim = core * 2 + head
        own = aim == y
        sp = jnp.where(own, me, z * NY + aim)
        tp = jnp.where(own, sibling, place * 2 + half)
        return pltpu.make_async_remote_copy(
            src_ref=kv_own.at[head, half], dst_ref=kv_all.at[me, half],
            send_sem=kv_send.at[head, half], recv_sem=kv_recv.at[me, half],
            device_id=(sp, tp), device_id_type=MESH,
        )

    def ring_copy(block, way):
        peer = lax.rem(z + (1 if way == 0 else NZ - 1), NZ) * NY + y
        return pltpu.make_async_remote_copy(
            src_ref=kv_all.at[block, core], dst_ref=kv_all.at[block, core],
            send_sem=ring_send.at[block, way], recv_sem=kv_recv.at[block, core],
            device_id=(peer, col), device_id_type=MESH,
        )

    def share_copy(block):
        return pltpu.make_async_remote_copy(
            src_ref=kv_all.at[block, core], dst_ref=kv_all.at[block, core],
            send_sem=share_send.at[block], recv_sem=kv_recv.at[block, core],
            device_id=(me, sibling), device_id_type=MESH,
        )

    def rows_of(to_z, to_core, block):
        return lax.rem(2 * to_z + to_core + 2 * block, SHARES)

    def q_copy(head, step):
        to_z, to_core = step // 2, lax.rem(step, 2)
        return pltpu.make_async_remote_copy(
            src_ref=q_own.at[head, rows_of(to_z, to_core, me)], dst_ref=q_all.at[me],
            send_sem=q_send.at[head, step], recv_sem=q_recv.at[me],
            device_id=(to_z * NY + core * 2 + head, place * 2 + to_core), device_id_type=MESH,
        )

    def q_here(head, step):
        to_z, to_core = step // 2, lax.rem(step, 2)
        return jnp.logical_and(to_z * NY + core * 2 + head == me, to_core == core)

    def back_owner(block):
        return lax.rem(z + block, n_tp)

    my_slot = (place * NY + y) * 2 + core

    def back_here(block):
        return jnp.logical_and(block == me, back_owner(block) == col)

    def back_copy(block):
        return pltpu.make_async_remote_copy(
            src_ref=packed.at[block], dst_ref=att.at[my_slot],
            send_sem=back_send.at[block], recv_sem=back_recv.at[my_slot],
            device_id=(block, back_owner(block)), device_id_type=MESH,
        )

    for copy in loads:
        copy.wait()
    for part in range(PARTS):
        for k in range(1, places):
            block = same_core(k)
            arrived(tok.at[block, part], tok_recv.at[block, part])
            token_copy(places + k - 1, part).start()
        arrived(tok.at[sibling, part], tok_recv.at[sibling, part])
        for k in range(1, places):
            block = lax.rem(place + k, places) * 2 + 1 - core
            arrived(tok.at[block, part], tok_recv.at[block, part])
        x = tok[:, part]
        depth = x.shape[1]
        both = jnp.dot(
            x.reshape(n_tp * depth, x.shape[2]), wqkv[...], preferred_element_type=F32
        )
        proj[:, part * depth : (part + 1) * depth, :] = both.reshape(n_tp, depth, 3 * LANES)
    for kind in range(places):
        wo_copy(kind).start()

    def turn(value):
        return pltpu.roll(value, DIM, 1)

    lane16 = lax.broadcasted_iota(jnp.int32, (16, LANES), 1)

    def weave(upper, lower):
        first = jnp.where(lane16 < DIM, upper, turn(lower)).astype(BF16)
        second = jnp.where(lane16 < DIM, turn(upper), lower).astype(BF16)
        return first, second

    def strided(i, kind):
        return proj[:, RUN - 1 - i, kind * LANES : (kind + 1) * LANES]

    for i in range(0, RUN // 2, 2):
        upper = jnp.concatenate([strided(i, 1), strided(i + 1, 1)], axis=0)
        lower = jnp.concatenate([strided(i + 32, 1), strided(i + 33, 1)], axis=0)
        kv_own[0, 0, 8 * i : 8 * i + 16], kv_own[1, 0, 8 * i : 8 * i + 16] = weave(upper, lower)
    for half in range(1):
        for head in range(2):
            kv_copy(head, half).start()
    for piece in range(4):
        block = jnp.concatenate([strided(16 * piece + i, 2) for i in range(16)], axis=0)
        flipped = block.T.astype(BF16)
        for head in range(2):
            kv_own[head, 1, DIM * piece : DIM * (piece + 1)] = flipped[DIM * head : DIM * (head + 1)]
    for head in range(2):
        kv_copy(head, 1).start()

    for share in range(SHARES):
        block, first = share // 2, 32 * (share % 2)
        q = proj[block, first : first + 32, 0:LANES] * (LOG2E * DIM ** (-0.5))
        q_own[0, share], q_own[1, share] = weave(q[:16], q[16:])

    def send_q(step, carry):
        for head in range(2):

            @pl.when(jnp.logical_not(q_here(head, step)))
            def _():
                q_copy(head, step).start()

        return carry

    lax.fori_loop(0, 2 * NZ, send_q, 0)

    for head in range(2):

        @pl.when(core * 2 + head == y)
        def _():
            kv_all[me] = kv_own[head]
            q_all[me] = q_own[head, rows_of(z, core, me)]

    def pass_on(block, step, sign):
        if step == 0:

            @pl.when(block != me)
            def _():
                arrived(kv_all.at[block, core], kv_recv.at[block, core])
                share_copy(block).start()

            @pl.when(jnp.logical_and(block == me, jnp.logical_not(mine)))
            def _():
                arrived(kv_all.at[block, core], kv_recv.at[block, core])

            for way in range(2):
                ring_copy(block, way).start()
        else:
            arrived(kv_all.at[block, core], kv_recv.at[block, core])
            share_copy(block).start()

    def group_at(offset):
        return lax.rem(z + offset + NZ, NZ)

    for part in range(NY):
        block = z * NY + part
        pass_on(block, 0, 0)

    def take_q(block, carry):
        @pl.when(jnp.logical_not(jnp.logical_and(block == me, mine)))
        def _():
            arrived(q_all.at[block], q_recv.at[block])

        return carry

    lax.fori_loop(0, n_sp, take_q, 0)

    def build(tile, carry):
        pieces = []
        for part in range(NY):
            pair = q_all[tile * NY + part].astype(F32)
            pieces.append(jnp.where(lane16 < DIM, pair, 0.0))
            pieces.append(jnp.where(lane16 < DIM, turn(pair), 0.0))
        flipped = jnp.concatenate(pieces, axis=0).T
        q_top[tile] = flipped.astype(BF16)
        q_low[tile] = jnp.concatenate([flipped[DIM:], flipped[:DIM]], axis=0).astype(BF16)
        return carry

    lax.fori_loop(0, TILES, build, 0)
    arrived(bias_all.at[1 - core], bias_recv)

    def suffix(keep):
        row = lax.broadcasted_iota(jnp.int32, keep.shape, 0)
        product = keep
        for step in (1, 2, 4):
            moved = pltpu.roll(product, 8 - step, 0)
            product = product * jnp.where(row + step < 8, moved, 1.0)
        after = jnp.where(row + 1 < 8, pltpu.roll(product, 7, 0), 1.0)
        return after, product[0:1]

    def segment(block, slot, q, width, bias, reach):
        scores = jnp.dot(kv_all[block, 0], q, preferred_element_type=F32)
        keep = jnp.ones((8, 2 * width), F32)
        for i in range(RUN // 2):
            score = scores[8 * i : 8 * i + 8] + bias
            if reach is not None:
                score = jnp.where(reach > -i, score, DEAD)
            odds = jnp.exp2(jnp.minimum(score, EXP_MAX))
            lose = 1.0 / (1.0 + odds)
            xs[slot, 8 * i : 8 * i + 8, 0 : 2 * width] = odds * lose * keep
            keep = keep * lose
        near, far = keep[:, :width], keep[:, width:]
        after, whole = suffix(near * far)
        values = kv_all[block, 1]
        out = None
        for half, factor in enumerate((after, after * near)):
            part = xs[slot, :, half * width : (half + 1) * width].reshape(RUN // 2, 8, width)
            weight = (part * factor[None]).reshape(HALF, width).astype(BF16)
            first = 2 * half * DIM
            value = jnp.concatenate(
                [values[first : first + DIM], values[first + DIM : first + 2 * DIM]], axis=1
            )
            term = jnp.dot(value, weight, preferred_element_type=F32)
            out = term if out is None else out + term
        return out, whole

    def cover(group, tile, count, diagonal):
        width = count * LANES
        q = jnp.concatenate(
            [q_top[tile + n] for n in range(count)] + [q_low[tile + n] for n in range(count)],
            axis=1,
        )
        bias = bias_all[head_core, head_local]
        bias = jnp.concatenate([bias] * (2 * count), axis=1)
        if diagonal:
            lane = lax.broadcasted_iota(jnp.int32, (8, 2 * width), 1)
            row = lax.broadcasted_iota(jnp.int32, (8, 2 * width), 0)
            half = lane // width
            inside = lax.rem(lane, width)
            part = lax.rem(inside // SHARE, NY)
            share = rows_of(z, core, tile * NY + part)
            query = SEG * part + SHARE * share + lax.rem(inside, SHARE)
            query = jnp.where(inside < LANES, query, FAR)
            reach = query - row * RUN - (RUN - 1) + half * (RUN // 2)
        acc = keep = None
        for part in range(NY):
            limit = reach - SEG * part if diagonal else None
            out, whole = segment(group * NY + part, part, q, width, bias, limit)
            acc = out if acc is None else acc * whole + out
            keep = whole if keep is None else keep * whole
        for n in range(count):
            seg_acc[group, tile + n] = acc[:, n * LANES : (n + 1) * LANES]
            seg_keep[group, tile + n] = jnp.broadcast_to(
                keep[:, n * LANES : (n + 1) * LANES], (8, LANES)
            )

    def attend(group):
        count = TILES - group
        odd = lax.rem(count, 2)

        @pl.when(odd == 1)
        def _():
            cover(group, group, 1, True)

        @pl.when(odd == 0)
        def _():
            cover(group, group, 2, True)

        def pair(step, carry):
            cover(group, group + 2 - odd + 2 * step, 2, False)
            return carry

        lax.fori_loop(0, (count - 1) // 2, pair, 0)

    def visit(step, carry):
        distance = (step + 1) // 2
        back = lax.rem(step, 2)
        group = lax.rem(z + NZ + jnp.where(back == 1, -distance, distance), NZ)

        @pl.when(jnp.logical_and(step > 0, step < NZ - 1))
        def _():
            for part in range(NY):
                block = group * NY + part
                arrived(kv_all.at[block, core], kv_recv.at[block, core])
                for way in range(2):
                    last = (part < NY // 2) == (way == 0)

                    @pl.when(
                        jnp.logical_and(back == 1 - way, distance < (4 if last else 3))
                    )
                    def _():
                        ring_copy(block, way).start()

                share_copy(block).start()

        @pl.when(step == NZ - 1)
        def _():
            for part in range(NY):
                block = group * NY + part
                arrived(kv_all.at[block, core], kv_recv.at[block, core])
                share_copy(block).start()
            for k in range(1, places):
                arrived(wfull.at[same_core(k)], wo_recv.at[same_core(k)])
                wo_copy(places + k - 1).start()

        for part in range(NY):
            block = group * NY + part

            @pl.when(jnp.logical_not(jnp.logical_and(block == me, mine)))
            def _():
                arrived(kv_all.at[block, 1 - core], kv_recv.at[block, 1 - core])

        attend(group)
        return carry

    lax.fori_loop(0, NZ, visit, 0)

    def combine(tile):
        def add(group, acc):
            return acc * seg_keep[group, tile][0:1] + seg_acc[group, tile]

        return lax.fori_loop(0, tile + 1, add, jnp.zeros((DIM, LANES), F32))

    def deliver(pair, carry):
        flipped = jnp.concatenate([combine(2 * pair), combine(2 * pair + 1)], axis=0).T
        for part in range(NY):
            upper = flipped[SHARE * part : SHARE * part + 16]
            lower = flipped[SHARE * part + 16 : SHARE * (part + 1)]
            for n, folded in enumerate(weave(upper, lower)):
                block = (2 * pair + n) * NY + part
                packed[block] = folded
                here = back_here(block)

                @pl.when(here)
                def _():
                    att[my_slot] = folded

                @pl.when(jnp.logical_not(here))
                def _():
                    back_copy(block).start()

        return carry

    lax.fori_loop(0, TILES // 2, deliver, 0)

    source_z = lax.rem(col + n_sp - me, NZ)
    for pair in range(n_tp):
        for sub in range(2):
            values = []
            for head in (2 * pair, 2 * pair + 1):
                slot = head * 2 + sub
                here = jnp.logical_and(source_z * NY + head % NY == me, 2 * (head // NY) + sub == col)

                @pl.when(jnp.logical_not(here))
                def _():
                    arrived(att.at[slot], back_recv.at[slot])

                values.append(att[slot].astype(F32))
            top = jnp.where(lane16 < DIM, values[0], turn(values[1]))
            low = jnp.where(lane16 < DIM, turn(values[0]), values[1])
            cols = slice(pair * LANES, (pair + 1) * LANES)
            att_rows[SHARE * sub : SHARE * sub + 16, cols] = top.astype(BF16)
            att_rows[SHARE * sub + 16 : SHARE * (sub + 1), cols] = low.astype(BF16)

    arrived(wfull.at[sibling], wo_recv.at[sibling])
    for k in range(1, places):
        block = lax.rem(place + k, places) * 2 + 1 - core
        arrived(wfull.at[block], wo_recv.at[block])
    for first in range(0, out_ref.shape[1], COLS):
        w = wfull[:, :, first : first + COLS].reshape(att_rows.shape[1], COLS)
        out_ref[:, first : first + COLS] = jnp.dot(
            att_rows[...], w, preferred_element_type=F32
        ).astype(BF16)

    bias_copy.wait_send()
    for kind in range(2 * places - 1):
        wo_copy(kind).wait_send()
        for part in range(PARTS):
            token_copy(kind, part).wait_send()
    for head in range(2):
        for half in range(2):
            kv_copy(head, half).wait_send()

    def drain_q(step, carry):
        for head in range(2):

            @pl.when(jnp.logical_not(q_here(head, step)))
            def _():
                q_copy(head, step).wait_send()

        return carry

    lax.fori_loop(0, 2 * NZ, drain_q, 0)

    def drain(block, carry):
        ahead = lax.rem(z - block // NY + NZ, NZ)
        behind = lax.rem(NZ - ahead, NZ)
        first = lax.rem(block, NY) < NY // 2

        @pl.when(jnp.logical_or(ahead < 3, jnp.logical_and(ahead == 3, first)))
        def _():
            ring_copy(block, 0).wait_send()

        @pl.when(
            jnp.logical_or(behind < 3, jnp.logical_and(behind == 3, jnp.logical_not(first)))
        )
        def _():
            ring_copy(block, 1).wait_send()

        @pl.when(block != me)
        def _():
            share_copy(block).wait_send()

        @pl.when(jnp.logical_not(back_here(block)))
        def _():
            back_copy(block).wait_send()

        return carry

    lax.fori_loop(0, n_sp, drain, 0)


def shards(tokens, w_query, w_key, w_value, head_bias, w_out):
    model, local_width = w_query.shape
    n_tp = lax.axis_size("tp")
    n_sp = lax.axis_size("sp")
    device_rows = tokens.shape[0]
    out_width = w_out.shape[1]
    kinds = n_tp - 1

    smem = pl.BlockSpec(memory_space=pltpu.SMEM)
    anywhere = pl.BlockSpec(memory_space=pl.ANY)
    dma = pltpu.SemaphoreType.DMA

    def vmem(*shape):
        return pltpu.VMEM(shape, BF16)

    return pl.pallas_call(
        layer_kernel,
        out_shape=jax.ShapeDtypeStruct((device_rows, out_width), BF16),
        in_specs=[smem] + [anywhere] * 5,
        out_specs=pl.BlockSpec(memory_space=pltpu.VMEM),
        scratch_shapes=[
            vmem(n_tp, PARTS, device_rows // PARTS, model),
            vmem(model, 3 * local_width),
            vmem(n_tp, local_width, out_width),
            pltpu.VMEM((n_tp, device_rows, 3 * local_width), F32),
            pltpu.VMEM((2, 2, 8, LANES), F32),
            vmem(2, 2, HALF, LANES),
            vmem(2, SHARES, SHARE // 2, LANES),
            vmem(n_sp, SHARE // 2, LANES),
            vmem(n_sp, 2, HALF, LANES),
            vmem(TILES, LANES, LANES),
            vmem(TILES, LANES, LANES),
            pltpu.VMEM((NY, HALF, 4 * LANES), F32),
            pltpu.VMEM((NZ, TILES, DIM, LANES), F32),
            pltpu.VMEM((NZ, TILES, 8, LANES), F32),
            vmem(n_sp, SHARE // 2, LANES),
            vmem(32, SHARE // 2, LANES),
            vmem(device_rows, n_tp * local_width),
            dma((5,)),
            dma((kinds, PARTS)),
            dma((n_tp, PARTS)),
            dma((kinds,)),
            dma((n_tp,)),
            dma,
            dma,
            dma((2, 2)),
            dma((n_sp, 2)),
            dma((n_sp, 2)),
            dma((n_sp,)),
            dma((2, 2 * NZ)),
            dma((n_sp,)),
            dma((n_sp,)),
            dma((32,)),
        ],
        compiler_params=pltpu.CompilerParams(
            collective_id=0, has_side_effects=True, vmem_limit_bytes=60 * 2**20
        ),
        name="layer",
    )(
        head_bias,
        tokens.reshape(PARTS, device_rows // PARTS, model),
        w_query, w_key, w_value, w_out,
    )


def solution(mesh):
    placed = (
        P(("sp", "tp"), None),
        P(None, "tp"),
        P(None, "tp"),
        P(None, "tp"),
        P("tp"),
        P("tp", None),
    )
    return jax.shard_map(
        shards, mesh=mesh, in_specs=placed, out_specs=P(("sp", "tp"), None), check_vma=False
    )
```

time: 408 us -> 95.6 us (0.23)
  the two profiles are of different devices: /device:TPU:249 before, /device:TPU:25 now
where the time goes in v1:
time: 95.6 us; the launch traced here: 93.9 us
  Pallas kernels  92.2 us (96%)
  local copies, waits for them, and re-layouts  1.67 us (2%)
    pallas_call x1, Pallas kernels, shards(): pl.pallas_call(layer_kernel, out_shape=jax.ShapeDtypeStruct((device_rows,...  92.2 us

profile of v1, /device:TPU:25, one launch (start us, length us, event | category | flops | bytes accessed | tf_op | source)
XLA Modules:
  0.0 93.9 jit_solution(4456693400607895709)
XLA Ops:
  0.0 92.2 %layer.1 = bf16[64,2048]{1,0:T(8,128)(2,1)} custom-call(f32[2]{0:T(128)} %bias_ref.1, bf16[4,16,2048]{2,1,0:T(8,128)(2,1)} %bitcast.1, bf16[2048,128]{1,0:T(8,128)(2,1)} %wq_ref.1, bf16[2048,128]{1,0:T(8,128)(2,1)} %wk_ref.1, bf16[2048,128]{1,0:T(8,128)(2,1)} %wv_ref.1, bf16[128,2048]{1,0:T(8,128)(2,1)} %wo_ref.1), custom_call_target="tpu_custom_call" | custom-call | tf_op jit(solution)/shard_map/layer/pallas_call | solution.py:541
  92.3 1.7 %copy.8 = bf16[64,2048]{1,0:T(8,128)(2,1)} copy(bf16[64,2048]{1,0:T(8,128)(2,1)} %layer.1) | data formatting | bytes 524288

commit v2 on v1

v2 whole, which is shorter than its diff:
```python
import functools
import math

import jax
import jax.numpy as jnp
from jax import lax
from jax.experimental import pallas as pl
from jax.experimental.pallas import tpu as pltpu
from jax.sharding import PartitionSpec as P

MESH = pl.DeviceIdType.MESH
F32, BF16 = jnp.float32, jnp.bfloat16
LOG2E = math.log2(math.e)
PARTS = 4
COLS = 512
EXP_MAX = 126.0
DEAD = -1e30
NZ, NY = 8, 4
SEG = 512
HALF = 256
LANES = 128
DIM = 64
RUN = 64
SHARE = 32
SHARES = SEG // SHARE
TILES = 8
FAR = 1 << 20
BATCH = 2
STEPS = NZ * NY // BATCH


def layer_kernel(
    bias_ref, tokens_ref, wq_ref, wk_ref, wv_ref, wo_ref, out_ref,
    tok, wqkv, wfull, proj, bias_all, kv_own, q_own, q_all, kv_all, q_top, q_low, raw, xs,
    seg_acc, seg_keep, packed, att, att_rows,
    plane_sem, load_sem, tok_send, tok_recv, wo_send, wo_recv, bias_send, bias_recv, kv_send, kv_recv,
    ring_send, share_send, q_send, q_recv, back_send, back_recv,
):
    me = lax.axis_index("sp")
    col = lax.axis_index("tp")
    n_sp, n_tp = NZ * NY, 8
    z, y = me // NY, lax.rem(me, NY)
    place, core = col // 2, lax.rem(col, 2)
    places = n_tp // 2
    sibling = place * 2 + 1 - core
    head_core, head_local = y // 2, lax.rem(y, 2)
    mine = core == head_core

    loads = [
        pltpu.make_async_copy(src, dst, load_sem.at[index])
        for index, (src, dst) in enumerate(
            [
                (tokens_ref, tok.at[col]),
                (wq_ref, wqkv.at[:, 0:LANES]),
                (wk_ref, wqkv.at[:, LANES : 2 * LANES]),
                (wv_ref, wqkv.at[:, 2 * LANES : 3 * LANES]),
                (wo_ref, wfull.at[col]),
            ]
        )
    ]
    for copy in loads:
        copy.start()

    barrier = pltpu.get_barrier_semaphore()
    for step in range(1, n_tp):
        pl.semaphore_signal(
            barrier, inc=1, device_id=(me, lax.rem(col + step, n_tp)), device_id_type=MESH
        )
    for step in range(1, NY):
        peer = z * NY + lax.rem(y + step, NY)
        for other in range(2):
            pl.semaphore_signal(
                barrier, inc=1, device_id=(peer, place * 2 + other), device_id_type=MESH
            )
    for step in range(1, NZ):
        peer = lax.rem(z + step, NZ) * NY + y
        pl.semaphore_signal(barrier, inc=1, device_id=(peer, col), device_id_type=MESH)
    for head in range(2):
        bias_all[core, head] = jnp.full((8, LANES), bias_ref[head] * LOG2E, F32)
    seg_acc[...] = jnp.zeros_like(seg_acc)
    seg_keep[...] = jnp.ones_like(seg_keep)
    pl.semaphore_wait(barrier, n_tp - 1 + 2 * (NY - 1) + NZ - 1)
    for step in range(1, NZ):
        peer = lax.rem(z + step, NZ) * NY + y
        pl.semaphore_signal(plane_sem, inc=1, device_id=(peer, col), device_id_type=MESH)

    def same_core(k):
        return lax.rem(place + k, places) * 2 + core

    def arrived(ref, sem):
        pltpu.make_async_copy(ref, ref, sem).wait()

    def link(kind, own, kept, sent, received, part):
        if kind == 2:
            ahead = part < PARTS // 2
            block = same_core(3 if ahead else 1)
            src, target = kept.at[block, part], same_core(1 if ahead else 3)
        elif kind < places:
            src, block = own.at[part], col
            target = sibling if kind == 0 else same_core(kind)
        else:
            block = same_core(kind - places + 1)
            src, target = kept.at[block, part], sibling
        return pltpu.make_async_remote_copy(
            src_ref=src, dst_ref=kept.at[block, part],
            send_sem=sent.at[kind, part], recv_sem=received.at[block, part],
            device_id=(me, target), device_id_type=MESH,
        )

    def token_copy(kind, part):
        return link(kind, tokens_ref, tok, tok_send, tok_recv, part)

    def wo_copy(kind, part):
        return link(kind, wo_ref, wfull, wo_send, wo_recv, part)

    def relay(copy, kept, received, part, k):
        block = same_core(k)
        arrived(kept.at[block, part], received.at[block, part])
        copy(places + k - 1, part).start()
        if k != 2 and (part < PARTS // 2) == (k == 3):
            copy(2, part).start()

    bias_copy = pltpu.make_async_remote_copy(
        src_ref=bias_all.at[core], dst_ref=bias_all.at[core],
        send_sem=bias_send, recv_sem=bias_recv, device_id=(me, sibling), device_id_type=MESH,
    )

    turned = (2, 3, 0, 1)
    for part in range(PARTS):
        token_copy(1, part).start()
        token_copy(3, turned[part]).start()
        token_copy(0, part).start()
    bias_copy.start()

    def kv_copy(head, half, stage):
        aim = core * 2 + head
        own = aim == y
        sp = jnp.where(own, me, z * NY + aim)
        tp = jnp.where(own, sibling, place * 2 + half)
        return pltpu.make_async_remote_copy(
            src_ref=kv_own.at[head, half, pl.ds(LANES * (1 - stage), LANES)],
            dst_ref=kv_all.at[me, half, pl.ds(LANES * (1 - stage), LANES)],
            send_sem=kv_send.at[head, half, stage], recv_sem=kv_recv.at[me, half],
            device_id=(sp, tp), device_id_type=MESH,
        )

    def ring_copy(block, way):
        peer = lax.rem(z + (1 if way == 0 else NZ - 1), NZ) * NY + y
        return pltpu.make_async_remote_copy(
            src_ref=kv_all.at[block, core], dst_ref=kv_all.at[block, core],
            send_sem=ring_send.at[block, way], recv_sem=kv_recv.at[block, core],
            device_id=(peer, col), device_id_type=MESH,
        )

    def share_copy(block):
        return pltpu.make_async_remote_copy(
            src_ref=kv_all.at[block, core], dst_ref=kv_all.at[block, core],
            send_sem=share_send.at[block], recv_sem=kv_recv.at[block, core],
            device_id=(me, sibling), device_id_type=MESH,
        )

    def rows_of(to_z, to_core, block):
        return lax.rem(2 * to_z + to_core + 2 * block, SHARES)

    def q_copy(head, step):
        to_z, to_core = step // 2, lax.rem(step, 2)
        return pltpu.make_async_remote_copy(
            src_ref=q_own.at[head, rows_of(to_z, to_core, me)], dst_ref=q_all.at[me],
            send_sem=q_send.at[head, step], recv_sem=q_recv.at[me],
            device_id=(to_z * NY + core * 2 + head, place * 2 + to_core), device_id_type=MESH,
        )

    def q_here(head, step):
        to_z, to_core = step // 2, lax.rem(step, 2)
        return jnp.logical_and(to_z * NY + core * 2 + head == me, to_core == core)

    def back_owner(block):
        return lax.rem(z + block, n_tp)

    my_slot = (place * NY + y) * 2 + core

    def back_here(block):
        return jnp.logical_and(block == me, back_owner(block) == col)

    def back_copy(block):
        return pltpu.make_async_remote_copy(
            src_ref=packed.at[block], dst_ref=att.at[my_slot],
            send_sem=back_send.at[block], recv_sem=back_recv.at[my_slot],
            device_id=(block, back_owner(block)), device_id_type=MESH,
        )

    for copy in loads:
        copy.wait()
    def turn(value):
        return pltpu.roll(value, DIM, 1)

    lane16 = lax.broadcasted_iota(jnp.int32, (16, LANES), 1)

    def weave(upper, lower):
        first = jnp.where(lane16 < DIM, upper, turn(lower)).astype(BF16)
        second = jnp.where(lane16 < DIM, turn(upper), lower).astype(BF16)
        return first, second

    def strided(i, kind):
        return proj[:, RUN - 1 - i, kind * LANES : (kind + 1) * LANES]

    for part in range(PARTS):
        relay(token_copy, tok, tok_recv, part, 3)
        relay(token_copy, tok, tok_recv, turned[part], 1)
    for stage in range(2):
        parts = (stage, stage + 2)
        for part in parts:
            relay(token_copy, tok, tok_recv, part, 2)
        for part in parts:
            arrived(tok.at[sibling, part], tok_recv.at[sibling, part])
            for k in range(1, places):
                block = lax.rem(place + k, places) * 2 + 1 - core
                arrived(tok.at[block, part], tok_recv.at[block, part])
        depth, model = tok.shape[2:]
        x = jnp.concatenate([tok[:, part].reshape(n_tp * depth, model) for part in parts], axis=0)
        both = jnp.dot(x, wqkv[...], preferred_element_type=F32)
        for index, part in enumerate(parts):
            proj[:, part * depth : (part + 1) * depth, :] = both[
                index * n_tp * depth : (index + 1) * n_tp * depth
            ].reshape(n_tp, depth, 3 * LANES)
        base = 16 * (1 - stage)
        for i in range(base, base + 16, 2):
            upper = jnp.concatenate([strided(i, 1), strided(i + 1, 1)], axis=0)
            lower = jnp.concatenate([strided(i + 32, 1), strided(i + 33, 1)], axis=0)
            kv_own[0, 0, 8 * i : 8 * i + 16], kv_own[1, 0, 8 * i : 8 * i + 16] = weave(
                upper, lower
            )
        for head in range(2):
            kv_copy(head, 0, stage).start()
        for index in range(2):
            first = base + 32 * index
            block = jnp.concatenate([strided(first + i, 2) for i in range(16)], axis=0)
            flipped = block.T.astype(BF16)
            at = LANES * (1 - stage) + DIM * index
            for head in range(2):
                kv_own[head, 1, at : at + DIM] = flipped[DIM * head : DIM * (head + 1)]
        for head in range(2):
            kv_copy(head, 1, stage).start()

    for part in range(PARTS):
        for kind in (1, 3, 0):
            wo_copy(kind, turned[part] if kind == 3 else part).start()

    for share in range(SHARES):
        block, first = share // 2, 32 * (share % 2)
        q = proj[block, first : first + 32, 0:LANES] * (LOG2E * DIM ** (-0.5))
        q_own[0, share], q_own[1, share] = weave(q[:16], q[16:])

    pl.semaphore_wait(plane_sem, NZ - 1)

    def send_q(step, carry):
        for head in range(2):

            @pl.when(jnp.logical_not(q_here(head, step)))
            def _():
                q_copy(head, step).start()

        return carry

    lax.fori_loop(0, 2 * NZ, send_q, 0)

    for head in range(2):

        @pl.when(core * 2 + head == y)
        def _():
            kv_all[me] = kv_own[head]
            q_all[me] = q_own[head, rows_of(z, core, me)]

    for part in range(NY):
        block = z * NY + part

        @pl.when(jnp.logical_not(jnp.logical_and(block == me, mine)))
        def _():
            arrived(kv_all.at[block, core], kv_recv.at[block, core])

        for way in range(2):
            ring_copy(block, way).start()

        @pl.when(block != me)
        def _():
            share_copy(block).start()

    def take_q(block, carry):
        @pl.when(jnp.logical_not(jnp.logical_and(block == me, mine)))
        def _():
            arrived(q_all.at[block], q_recv.at[block])

        return carry

    lax.fori_loop(0, n_sp, take_q, 0)

    def build(tile, carry):
        pieces = []
        for part in range(NY):
            pair = q_all[tile * NY + part].astype(F32)
            pieces.append(jnp.where(lane16 < DIM, pair, 0.0))
            pieces.append(jnp.where(lane16 < DIM, turn(pair), 0.0))
        flipped = jnp.concatenate(pieces, axis=0).T
        q_top[tile] = flipped.astype(BF16)
        q_low[tile] = jnp.concatenate([flipped[DIM:], flipped[:DIM]], axis=0).astype(BF16)
        return carry

    lax.fori_loop(0, TILES, build, 0)
    arrived(bias_all.at[1 - core], bias_recv)

    def suffix(keep):
        row = lax.broadcasted_iota(jnp.int32, keep.shape, 0)
        product = keep
        for step in (1, 2, 4):
            moved = pltpu.roll(product, 8 - step, 0)
            product = product * jnp.where(row + step < 8, moved, 1.0)
        after = jnp.where(row + 1 < 8, pltpu.roll(product, 7, 0), 1.0)
        return after, product[0:1]

    def segment(block, slot, width, bias, reach):
        keep = jnp.ones((8, 2 * width), F32)
        for i in range(RUN // 2):
            score = raw[slot, 8 * i : 8 * i + 8, 0 : 2 * width] + bias
            if reach is not None:
                score = jnp.where(reach > -i, score, DEAD)
            odds = jnp.exp2(jnp.minimum(score, EXP_MAX))
            lose = 1.0 / (1.0 + odds)
            xs[slot, 8 * i : 8 * i + 8, 0 : 2 * width] = odds * lose * keep
            keep = keep * lose
        near, far = keep[:, :width], keep[:, width:]
        after, whole = suffix(near * far)
        values = kv_all[block, 1]
        out = None
        for half, factor in enumerate((after, after * near)):
            part = xs[slot, :, half * width : (half + 1) * width].reshape(RUN // 2, 8, width)
            weight = (part * factor[None]).reshape(HALF, width).astype(BF16)
            first = half * DIM
            value = jnp.concatenate(
                [values[first : first + DIM], values[LANES + first : LANES + first + DIM]], axis=1
            )
            term = jnp.dot(value, weight, preferred_element_type=F32)
            out = term if out is None else out + term
        return out, whole

    def cover(group, part, tile, count, diagonal):
        width = count * LANES
        q = jnp.concatenate(
            [q_top[tile + n] for n in range(count)] + [q_low[tile + n] for n in range(count)],
            axis=1,
        )
        bias = bias_all[head_core, head_local]
        bias = jnp.concatenate([bias] * (2 * count), axis=1)
        if diagonal:
            lane = lax.broadcasted_iota(jnp.int32, (8, 2 * width), 1)
            row = lax.broadcasted_iota(jnp.int32, (8, 2 * width), 0)
            half = lane // width
            inside = lax.rem(lane, width)
            owner = lax.rem(inside // SHARE, NY)
            share = rows_of(z, core, tile * NY + owner)
            query = SEG * owner + SHARE * share + lax.rem(inside, SHARE)
            query = jnp.where(inside < LANES, query, FAR)
            reach = query - row * RUN - (RUN - 1) + half * (RUN // 2) - SEG * part
        first = group * NY + part
        raw[:, :, 0 : 2 * width] = jnp.dot(
            kv_all[pl.ds(first, BATCH), 0].reshape(BATCH * HALF, LANES), q,
            preferred_element_type=F32,
        ).reshape(BATCH, HALF, 2 * width)
        acc = [seg_acc[group, tile + n] for n in range(count)]
        keep = [seg_keep[group, tile + n][0:1] for n in range(count)]
        for index in range(BATCH):
            limit = reach - SEG * index if diagonal else None
            out, whole = segment(first + index, index, width, bias, limit)
            for n in range(count):
                lanes = slice(n * LANES, (n + 1) * LANES)
                acc[n] = acc[n] * whole[:, lanes] + out[:, lanes]
                keep[n] = keep[n] * whole[:, lanes]
        for n in range(count):
            seg_acc[group, tile + n] = acc[n]
            seg_keep[group, tile + n] = jnp.broadcast_to(keep[n], (8, LANES))

    def attend(group, part):
        count = TILES - group
        odd = lax.rem(count, 2)

        @pl.when(odd == 1)
        def _():
            cover(group, part, group, 1, True)

        @pl.when(odd == 0)
        def _():
            cover(group, part, group, 2, True)

        def pair(step, carry):
            cover(group, part, group + 2 - odd + 2 * step, 2, False)
            return carry

        lax.fori_loop(0, (count - 1) // 2, pair, 0)

    def stop_at(step):
        turn_of = lax.rem(step + 2, 4)
        far = step >= STEPS - 2
        distance = (step + 2) // 4
        own = step < 2
        behind = jnp.logical_or(jnp.logical_and(far, turn_of == 0), lax.rem(step, 2) == 0)
        part = jnp.where(jnp.logical_or(own, far), lax.rem(step, 2), turn_of // 2) * BATCH
        group = lax.rem(z + NZ + jnp.where(behind, -distance, distance), NZ)
        return distance, behind, group, part

    def visit(step, carry):
        ahead = step + 1

        @pl.when(jnp.logical_and(ahead >= 2, ahead < STEPS))
        def _():
            distance, behind, group, part = stop_at(ahead)
            for index in range(BATCH):
                block = group * NY + part + index
                arrived(kv_all.at[block, core], kv_recv.at[block, core])

                @pl.when(
                    jnp.logical_and(
                        behind, jnp.logical_or(distance < 3, jnp.logical_and(distance == 3, part == 0))
                    )
                )
                def _():
                    ring_copy(block, 0).start()

                @pl.when(
                    jnp.logical_and(
                        jnp.logical_not(behind),
                        jnp.logical_or(distance < 3, jnp.logical_and(distance == 3, part > 0)),
                    )
                )
                def _():
                    ring_copy(block, 1).start()

                share_copy(block).start()

        @pl.when(step == STEPS // 2)
        def _():
            for part in range(PARTS):
                relay(wo_copy, wfull, wo_recv, part, 3)
                relay(wo_copy, wfull, wo_recv, turned[part], 1)

        @pl.when(step == STEPS - 2)
        def _():
            for part in range(PARTS):
                relay(wo_copy, wfull, wo_recv, part, 2)

        distance, behind, group, part = stop_at(step)
        for index in range(BATCH):
            block = group * NY + part + index

            @pl.when(jnp.logical_not(jnp.logical_and(block == me, mine)))
            def _():
                arrived(kv_all.at[block, 1 - core], kv_recv.at[block, 1 - core])

        attend(group, part)
        return carry

    lax.fori_loop(0, STEPS, visit, 0)

    def combine(tile):
        acc = seg_acc[0, tile]
        for group in range(1, NZ):
            acc = acc * seg_keep[group, tile][0:1] + seg_acc[group, tile]
        return acc

    def deliver(pair, carry):
        flipped = jnp.concatenate([combine(2 * pair), combine(2 * pair + 1)], axis=0).T
        for part in range(NY):
            upper = flipped[SHARE * part : SHARE * part + 16]
            lower = flipped[SHARE * part + 16 : SHARE * (part + 1)]
            for n, folded in enumerate(weave(upper, lower)):
                block = (2 * pair + n) * NY + part
                packed[block] = folded
                here = back_here(block)

                @pl.when(here)
                def _():
                    att[my_slot] = folded

                @pl.when(jnp.logical_not(here))
                def _():
                    back_copy(block).start()

        return carry

    lax.fori_loop(0, TILES // 2, deliver, 0)

    bias_copy.wait_send()
    for part in range(PARTS):
        for kind in range(2 * places - 1):
            wo_copy(kind, part).wait_send()
            token_copy(kind, part).wait_send()
    for head in range(2):
        for half in range(2):
            for stage in range(2):
                kv_copy(head, half, stage).wait_send()

    def drain_q(step, carry):
        for head in range(2):

            @pl.when(jnp.logical_not(q_here(head, step)))
            def _():
                q_copy(head, step).wait_send()

        return carry

    lax.fori_loop(0, 2 * NZ, drain_q, 0)

    def drain(block, carry):
        ahead = lax.rem(z - block // NY + NZ, NZ)
        behind = lax.rem(NZ - ahead, NZ)
        first = lax.rem(block, NY) < NY // 2

        @pl.when(jnp.logical_or(ahead < 3, jnp.logical_and(ahead == 3, first)))
        def _():
            ring_copy(block, 0).wait_send()

        @pl.when(
            jnp.logical_or(behind < 3, jnp.logical_and(behind == 3, jnp.logical_not(first)))
        )
        def _():
            ring_copy(block, 1).wait_send()

        @pl.when(block != me)
        def _():
            share_copy(block).wait_send()

        return carry

    lax.fori_loop(0, n_sp, drain, 0)

    source_z = lax.rem(col + n_sp - me, NZ)
    for pair in range(n_tp):
        for sub in range(2):
            values = []
            for head in (2 * pair, 2 * pair + 1):
                slot = head * 2 + sub
                here = jnp.logical_and(source_z * NY + head % NY == me, 2 * (head // NY) + sub == col)

                @pl.when(jnp.logical_not(here))
                def _():
                    arrived(att.at[slot], back_recv.at[slot])

                values.append(att[slot].astype(F32))
            top = jnp.where(lane16 < DIM, values[0], turn(values[1]))
            low = jnp.where(lane16 < DIM, turn(values[0]), values[1])
            cols = slice(pair * LANES, (pair + 1) * LANES)
            att_rows[SHARE * sub : SHARE * sub + 16, cols] = top.astype(BF16)
            att_rows[SHARE * sub + 16 : SHARE * (sub + 1), cols] = low.astype(BF16)

    for part in range(PARTS):
        arrived(wfull.at[sibling, part], wo_recv.at[sibling, part])
        for k in range(1, places):
            block = lax.rem(place + k, places) * 2 + 1 - core
            arrived(wfull.at[block, part], wo_recv.at[block, part])
    for first in range(0, out_ref.shape[1], COLS):
        w = wfull[:, :, :, first : first + COLS].reshape(att_rows.shape[1], COLS)
        out_ref[:, first : first + COLS] = jnp.dot(
            att_rows[...], w, preferred_element_type=F32
        ).astype(BF16)

    def drain_back(block, carry):
        @pl.when(jnp.logical_not(back_here(block)))
        def _():
            back_copy(block).wait_send()

        return carry

    lax.fori_loop(0, n_sp, drain_back, 0)


def shards(tokens, w_query, w_key, w_value, head_bias, w_out):
    model, local_width = w_query.shape
    n_tp = lax.axis_size("tp")
    n_sp = lax.axis_size("sp")
    device_rows = tokens.shape[0]
    out_width = w_out.shape[1]
    kinds = n_tp - 1

    smem = pl.BlockSpec(memory_space=pltpu.SMEM)
    anywhere = pl.BlockSpec(memory_space=pl.ANY)
    dma = pltpu.SemaphoreType.DMA

    def vmem(*shape):
        return pltpu.VMEM(shape, BF16)

    return pl.pallas_call(
        layer_kernel,
        out_shape=jax.ShapeDtypeStruct((device_rows, out_width), BF16),
        in_specs=[smem] + [anywhere] * 5,
        out_specs=pl.BlockSpec(memory_space=pltpu.VMEM),
        scratch_shapes=[
            vmem(n_tp, PARTS, device_rows // PARTS, model),
            vmem(model, 3 * local_width),
            vmem(n_tp, PARTS, local_width // PARTS, out_width),
            pltpu.VMEM((n_tp, device_rows, 3 * local_width), F32),
            pltpu.VMEM((2, 2, 8, LANES), F32),
            vmem(2, 2, HALF, LANES),
            vmem(2, SHARES, SHARE // 2, LANES),
            vmem(n_sp, SHARE // 2, LANES),
            vmem(n_sp, 2, HALF, LANES),
            vmem(TILES, LANES, LANES),
            vmem(TILES, LANES, LANES),
            pltpu.VMEM((BATCH, HALF, 4 * LANES), F32),
            pltpu.VMEM((BATCH, HALF, 4 * LANES), F32),
            pltpu.VMEM((NZ, TILES, DIM, LANES), F32),
            pltpu.VMEM((NZ, TILES, 8, LANES), F32),
            vmem(n_sp, SHARE // 2, LANES),
            vmem(32, SHARE // 2, LANES),
            vmem(device_rows, n_tp * local_width),
            pltpu.SemaphoreType.REGULAR,
            dma((5,)),
            dma((kinds, PARTS)),
            dma((n_tp, PARTS)),
            dma((kinds, PARTS)),
            dma((n_tp, PARTS)),
            dma,
            dma,
            dma((2, 2, 2)),
            dma((n_sp, 2)),
            dma((n_sp, 2)),
            dma((n_sp,)),
            dma((2, 2 * NZ)),
            dma((n_sp,)),
            dma((n_sp,)),
            dma((32,)),
        ],
        compiler_params=pltpu.CompilerParams(
            collective_id=0, has_side_effects=True, vmem_limit_bytes=60 * 2**20
        ),
        name="layer",
    )(
        head_bias,
        tokens.reshape(PARTS, device_rows // PARTS, model),
        w_query, w_key, w_value,
        w_out.reshape(PARTS, local_width // PARTS, out_width),
    )


def solution(mesh):
    placed = (
        P(("sp", "tp"), None),
        P(None, "tp"),
        P(None, "tp"),
        P(None, "tp"),
        P("tp"),
        P("tp", None),
    )
    return jax.shard_map(
        shards, mesh=mesh, in_specs=placed, out_specs=P(("sp", "tp"), None), check_vma=False
    )
```

time: 95.6 us -> 78 us (0.82)
  Pallas kernels: 92.2 us -> 75.4 us
    pallas_call x1, Pallas kernels: 92.2 us -> 75.4 us  [shards(): pl.pallas_call(layer_kernel, out_shape=jax.ShapeDtypeStruct((device_rows,...]
where the time goes in v2:
time: 78 us; the launch traced here: 77 us
  Pallas kernels  75.4 us (97%)
  local copies, waits for them, and re-layouts  1.67 us (2%)
    pallas_call x1, Pallas kernels, shards(): pl.pallas_call(layer_kernel, out_shape=jax.ShapeDtypeStruct((device_rows,...  75.4 us
    unnamed x1, local copies, waits for them, and re-layouts  1.67 us

profile of v2, /device:TPU:25, one launch (start us, length us, event | category | flops | bytes accessed | tf_op | source)
XLA Modules:
  0.0 77.0 jit_solution(10780277642969291968)
XLA Ops:
  0.0 75.4 %layer.1 = bf16[64,2048]{1,0:T(8,128)(2,1)} custom-call(f32[2]{0:T(128)} %bias_ref.1, bf16[4,16,2048]{2,1,0:T(8,128)(2,1)} %bitcast.3, bf16[2048,128]{1,0:T(8,128)(2,1)} %wq_ref.1, bf16[2048,128]{1,0:T(8,128)(2,1)} %wk_ref.1, bf16[2048,128]{1,0:T(8,128)(2,1)} %wv_ref.1, bf16[4,32,2048]{2,1,0:T(8,128)(2,1)} %bitcast.2), custom_call_target="tpu_custom_call" | custom-call | tf_op jit(solution)/shard_map/layer/pallas_call | solution.py:589
  75.4 1.7 %copy.8 = bf16[64,2048]{1,0:T(8,128)(2,1)} copy(bf16[64,2048]{1,0:T(8,128)(2,1)} %layer.1) | data formatting | bytes 524288

commit v3 on v2

--- a/solution.py
+++ b/solution.py
@@ -32,8 +32,8 @@
 def layer_kernel(
     bias_ref, tokens_ref, wq_ref, wk_ref, wv_ref, wo_ref, out_ref,
     tok, wqkv, wfull, proj, bias_all, kv_own, q_own, q_all, kv_all, q_top, q_low, raw, xs,
-    seg_acc, seg_keep, packed, att, att_rows,
-    plane_sem, load_sem, tok_send, tok_recv, wo_send, wo_recv, bias_send, bias_recv, kv_send, kv_recv,
+    seg_acc, seg_keep, packed, att, att_rows, mixed,
+    plane_sem, out_sem, load_sem, tok_send, tok_recv, wo_send, wo_recv, bias_send, bias_recv, kv_send, kv_recv,
     ring_send, share_send, q_send, q_recv, back_send, back_recv,
 ):
     me = lax.axis_index("sp")
@@ -126,9 +126,10 @@
     )
 
     turned = (2, 3, 0, 1)
-    for part in range(PARTS):
+    for part in range(PARTS // 2):
         token_copy(1, part).start()
         token_copy(3, turned[part]).start()
+    for part in (0, 2, 1, 3):
         token_copy(0, part).start()
     bias_copy.start()
 
@@ -204,11 +205,24 @@
     def strided(i, kind):
         return proj[:, RUN - 1 - i, kind * LANES : (kind + 1) * LANES]
 
-    for part in range(PARTS):
+    def send_q(step, carry):
+        for head in range(2):
+
+            @pl.when(jnp.logical_not(q_here(head, step)))
+            def _():
+                q_copy(head, step).start()
+
+        return carry
+
+    for part in range(PARTS // 2):
         relay(token_copy, tok, tok_recv, part, 3)
+        token_copy(1, part + 2).start()
         relay(token_copy, tok, tok_recv, turned[part], 1)
+        token_copy(3, turned[part + 2]).start()
     for stage in range(2):
         parts = (stage, stage + 2)
+        relay(token_copy, tok, tok_recv, stage + 2, 3)
+        relay(token_copy, tok, tok_recv, turned[stage + 2], 1)
         for part in parts:
             relay(token_copy, tok, tok_recv, part, 2)
         for part in parts:
@@ -223,6 +237,13 @@
             proj[:, part * depth : (part + 1) * depth, :] = both[
                 index * n_tp * depth : (index + 1) * n_tp * depth
             ].reshape(n_tp, depth, 3 * LANES)
+        if stage == 1:
+            for share in range(SHARES):
+                block, first = share // 2, 32 * (share % 2)
+                q = proj[block, first : first + 32, 0:LANES] * (LOG2E * DIM ** (-0.5))
+                q_own[0, share], q_own[1, share] = weave(q[:16], q[16:])
+            pl.semaphore_wait(plane_sem, NZ - 1)
+            lax.fori_loop(0, 2 * NZ, send_q, 0)
         base = 16 * (1 - stage)
         for i in range(base, base + 16, 2):
             upper = jnp.concatenate([strided(i, 1), strided(i + 1, 1)], axis=0)
@@ -246,24 +267,6 @@
         for kind in (1, 3, 0):
             wo_copy(kind, turned[part] if kind == 3 else part).start()
 
-    for share in range(SHARES):
-        block, first = share // 2, 32 * (share % 2)
-        q = proj[block, first : first + 32, 0:LANES] * (LOG2E * DIM ** (-0.5))
-        q_own[0, share], q_own[1, share] = weave(q[:16], q[16:])
-
-    pl.semaphore_wait(plane_sem, NZ - 1)
-
-    def send_q(step, carry):
-        for head in range(2):
-
-            @pl.when(jnp.logical_not(q_here(head, step)))
-            def _():
-                q_copy(head, step).start()
-
-        return carry
-
-    lax.fori_loop(0, 2 * NZ, send_q, 0)
-
     for head in range(2):
 
         @pl.when(core * 2 + head == y)
@@ -317,22 +320,22 @@
         after = jnp.where(row + 1 < 8, pltpu.roll(product, 7, 0), 1.0)
         return after, product[0:1]
 
-    def segment(block, slot, width, bias, reach):
+    def segment(block, bank, slot, width, bias, reach):
         keep = jnp.ones((8, 2 * width), F32)
         for i in range(RUN // 2):
-            score = raw[slot, 8 * i : 8 * i + 8, 0 : 2 * width] + bias
+            score = raw[bank, slot, 8 * i : 8 * i + 8, 0 : 2 * width] + bias
             if reach is not None:
                 score = jnp.where(reach > -i, score, DEAD)
             odds = jnp.exp2(jnp.minimum(score, EXP_MAX))
             lose = 1.0 / (1.0 + odds)
-            xs[slot, 8 * i : 8 * i + 8, 0 : 2 * width] = odds * lose * keep
+            xs[bank, slot, 8 * i : 8 * i + 8, 0 : 2 * width] = odds * lose * keep
             keep = keep * lose
         near, far = keep[:, :width], keep[:, width:]
         after, whole = suffix(near * far)
         values = kv_all[block, 1]
         out = None
         for half, factor in enumerate((after, after * near)):
-            part = xs[slot, :, half * width : (half + 1) * width].reshape(RUN // 2, 8, width)
+            part = xs[bank, slot, :, half * width : (half + 1) * width].reshape(RUN // 2, 8, width)
             weight = (part * factor[None]).reshape(HALF, width).astype(BF16)
             first = half * DIM
             value = jnp.concatenate(
@@ -342,7 +345,7 @@
             out = term if out is None else out + term
         return out, whole
 
-    def cover(group, part, tile, count, diagonal):
+    def cover(group, part, tile, count, diagonal, bank):
         width = count * LANES
         q = jnp.concatenate(
             [q_top[tile + n] for n in range(count)] + [q_low[tile + n] for n in range(count)],
@@ -361,7 +364,7 @@
             query = jnp.where(inside < LANES, query, FAR)
             reach = query - row * RUN - (RUN - 1) + half * (RUN // 2) - SEG * part
         first = group * NY + part
-        raw[:, :, 0 : 2 * width] = jnp.dot(
+        raw[bank, :, :, 0 : 2 * width] = jnp.dot(
             kv_all[pl.ds(first, BATCH), 0].reshape(BATCH * HALF, LANES), q,
             preferred_element_type=F32,
         ).reshape(BATCH, HALF, 2 * width)
@@ -369,7 +372,7 @@
         keep = [seg_keep[group, tile + n][0:1] for n in range(count)]
         for index in range(BATCH):
             limit = reach - SEG * index if diagonal else None
-            out, whole = segment(first + index, index, width, bias, limit)
+            out, whole = segment(first + index, bank, index, width, bias, limit)
             for n in range(count):
                 lanes = slice(n * LANES, (n + 1) * LANES)
                 acc[n] = acc[n] * whole[:, lanes] + out[:, lanes]
@@ -381,20 +384,26 @@
     def attend(group, part):
         count = TILES - group
         odd = lax.rem(count, 2)
-
-        @pl.when(odd == 1)
-        def _():
-            cover(group, part, group, 1, True)
-
-        @pl.when(odd == 0)
-        def _():
-            cover(group, part, group, 2, True)
-
-        def pair(step, carry):
-            cover(group, part, group + 2 - odd + 2 * step, 2, False)
-            return carry
-
-        lax.fori_loop(0, (count - 1) // 2, pair, 0)
+        pairs = (count - 1) // 2
+        first = group + 2 - odd
+
+        for single in range(2):
+            for more in range(2):
+
+                @pl.when(jnp.logical_and(odd == single, (pairs > 0) == (more == 1)))
+                def _():
+                    cover(group, part, group, 2 - single, True, 0)
+                    if more:
+                        cover(group, part, first, 2, False, 1)
+
+        @pl.when(pairs == 2)
+        def _():
+            cover(group, part, first + 2, 2, False, 0)
+
+        @pl.when(pairs == 3)
+        def _():
+            cover(group, part, first + 2, 2, False, 0)
+            cover(group, part, first + 4, 2, False, 1)
 
     def stop_at(step):
         turn_of = lax.rem(step + 2, 4)
@@ -531,6 +540,15 @@
 
     lax.fori_loop(0, n_sp, drain, 0)
 
+    def drain_back(block, carry):
+        @pl.when(jnp.logical_not(back_here(block)))
+        def _():
+            back_copy(block).wait_send()
+
+        return carry
+
+    lax.fori_loop(0, n_sp, drain_back, 0)
+
     source_z = lax.rem(col + n_sp - me, NZ)
     for pair in range(n_tp):
         for sub in range(2):
@@ -555,20 +573,21 @@
         for k in range(1, places):
             block = lax.rem(place + k, places) * 2 + 1 - core
             arrived(wfull.at[block, part], wo_recv.at[block, part])
+
+    def put(first):
+        return pltpu.make_async_copy(
+            mixed.at[:, pl.ds(first, COLS)], out_ref.at[:, pl.ds(first, COLS)],
+            out_sem.at[first // COLS],
+        )
+
     for first in range(0, out_ref.shape[1], COLS):
         w = wfull[:, :, :, first : first + COLS].reshape(att_rows.shape[1], COLS)
-        out_ref[:, first : first + COLS] = jnp.dot(
+        mixed[:, first : first + COLS] = jnp.dot(
             att_rows[...], w, preferred_element_type=F32
         ).astype(BF16)
-
-    def drain_back(block, carry):
-        @pl.when(jnp.logical_not(back_here(block)))
-        def _():
-            back_copy(block).wait_send()
-
-        return carry
-
-    lax.fori_loop(0, n_sp, drain_back, 0)
+        put(first).start()
+    for first in range(0, out_ref.shape[1], COLS):
+        put(first).wait()
 
 
 def shards(tokens, w_query, w_key, w_value, head_bias, w_out):
@@ -590,7 +609,7 @@
         layer_kernel,
         out_shape=jax.ShapeDtypeStruct((device_rows, out_width), BF16),
         in_specs=[smem] + [anywhere] * 5,
-        out_specs=pl.BlockSpec(memory_space=pltpu.VMEM),
+        out_specs=anywhere,
         scratch_shapes=[
             vmem(n_tp, PARTS, device_rows // PARTS, model),
             vmem(model, 3 * local_width),
@@ -603,14 +622,16 @@
             vmem(n_sp, 2, HALF, LANES),
             vmem(TILES, LANES, LANES),
             vmem(TILES, LANES, LANES),
-            pltpu.VMEM((BATCH, HALF, 4 * LANES), F32),
-            pltpu.VMEM((BATCH, HALF, 4 * LANES), F32),
+            pltpu.VMEM((2, BATCH, HALF, 4 * LANES), F32),
+            pltpu.VMEM((2, BATCH, HALF, 4 * LANES), F32),
             pltpu.VMEM((NZ, TILES, DIM, LANES), F32),
             pltpu.VMEM((NZ, TILES, 8, LANES), F32),
             vmem(n_sp, SHARE // 2, LANES),
             vmem(32, SHARE // 2, LANES),
             vmem(device_rows, n_tp * local_width),
+            vmem(device_rows, out_width),
             pltpu.SemaphoreType.REGULAR,
+            dma((out_width // COLS,)),
             dma((5,)),
             dma((kinds, PARTS)),
             dma((n_tp, PARTS)),

time: 78 us -> 75.3 us (0.965)
  Pallas kernels: 75.4 us -> 73 us
    pallas_call x1, Pallas kernels: 75.4 us -> 73 us  [shards(): pl.pallas_call(layer_kernel, out_shape=jax.ShapeDtypeStruct((device_rows,...]
where the time goes in v3:
time: 75.3 us; the launch traced here: 74.6 us
  Pallas kernels  73 us (97%)
  local copies, waits for them, and re-layouts  1.67 us (2%)
    pallas_call x1, Pallas kernels, shards(): pl.pallas_call(layer_kernel, out_shape=jax.ShapeDtypeStruct((device_rows,...  73 us
    unnamed x1, local copies, waits for them, and re-layouts  1.67 us

profile of v3, /device:TPU:25, one launch (start us, length us, event | category | flops | bytes accessed | tf_op | source)
XLA Modules:
  0.0 74.6 jit_solution(2045062933300947951)
XLA Ops:
  0.0 73.0 %layer.1 = bf16[64,2048]{1,0:T(8,128)(2,1)} custom-call(f32[2]{0:T(128)} %bias_ref.1, bf16[4,16,2048]{2,1,0:T(8,128)(2,1)} %bitcast.3, bf16[2048,128]{1,0:T(8,128)(2,1)} %wq_ref.1, bf16[2048,128]{1,0:T(8,128)(2,1)} %wk_ref.1, bf16[2048,128]{1,0:T(8,128)(2,1)} %wv_ref.1, bf16[4,32,2048]{2,1,0:T(8,128)(2,1)} %bitcast.2), custom_call_target="tpu_custom_call" | custom-call | tf_op jit(solution)/shard_map/layer/pallas_call | solution.py:608
  73.0 1.7 %copy.8 = bf16[64,2048]{1,0:T(8,128)(2,1)} copy(bf16[64,2048]{1,0:T(8,128)(2,1)} %layer.1) | data formatting | bytes 524288

commit v4 on v3

--- a/solution.py
+++ b/solution.py
@@ -33,8 +33,8 @@
     bias_ref, tokens_ref, wq_ref, wk_ref, wv_ref, wo_ref, out_ref,
     tok, wqkv, wfull, proj, bias_all, kv_own, q_own, q_all, kv_all, q_top, q_low, raw, xs,
     seg_acc, seg_keep, packed, att, att_rows, mixed,
-    plane_sem, out_sem, load_sem, tok_send, tok_recv, wo_send, wo_recv, bias_send, bias_recv, kv_send, kv_recv,
-    ring_send, share_send, q_send, q_recv, back_send, back_recv,
+    plane_sem, out_sem, load_sem, tok_send, tok_recv, tok_pair, wo_send, wo_recv, wo_pair,
+    bias_send, bias_recv, kv_send, kv_recv, ring_send, share_send, q_send, q_recv, back_send, back_recv,
 ):
     me = lax.axis_index("sp")
     col = lax.axis_index("tp")
@@ -90,9 +90,9 @@
     def arrived(ref, sem):
         pltpu.make_async_copy(ref, ref, sem).wait()
 
-    def link(kind, own, kept, sent, received, part):
+    def link(kind, own, kept, sent, received, paired, part):
         if kind == 2:
-            ahead = part < PARTS // 2
+            ahead = part < kept.shape[1] // 2
             block = same_core(3 if ahead else 1)
             src, target = kept.at[block, part], same_core(1 if ahead else 3)
         elif kind < places:
@@ -101,23 +101,24 @@
         else:
             block = same_core(kind - places + 1)
             src, target = kept.at[block, part], sibling
+        inside = kind == 0 or kind >= places
         return pltpu.make_async_remote_copy(
-            src_ref=src, dst_ref=kept.at[block, part],
-            send_sem=sent.at[kind, part], recv_sem=received.at[block, part],
+            src_ref=src, dst_ref=kept.at[block, part], send_sem=sent,
+            recv_sem=paired.at[part % 2] if inside else received.at[block // 2, part],
             device_id=(me, target), device_id_type=MESH,
         )
 
     def token_copy(kind, part):
-        return link(kind, tokens_ref, tok, tok_send, tok_recv, part)
+        return link(kind, tokens_ref, tok, tok_send, tok_recv, tok_pair, part)
 
     def wo_copy(kind, part):
-        return link(kind, wo_ref, wfull, wo_send, wo_recv, part)
+        return link(kind, wo_ref, wfull, wo_send, wo_recv, wo_pair, part)
 
     def relay(copy, kept, received, part, k):
         block = same_core(k)
-        arrived(kept.at[block, part], received.at[block, part])
+        arrived(kept.at[block, part], received.at[block // 2, part])
         copy(places + k - 1, part).start()
-        if k != 2 and (part < PARTS // 2) == (k == 3):
+        if k != 2 and (part < kept.shape[1] // 2) == (k == 3):
             copy(2, part).start()
 
     bias_copy = pltpu.make_async_remote_copy(
@@ -132,6 +133,9 @@
     for part in (0, 2, 1, 3):
         token_copy(0, part).start()
     bias_copy.start()
+
+    def pair_at(block):
+        return n_sp + block // BATCH
 
     def kv_copy(head, half, stage):
         aim = core * 2 + head
@@ -141,7 +145,10 @@
         return pltpu.make_async_remote_copy(
             src_ref=kv_own.at[head, half, pl.ds(LANES * (1 - stage), LANES)],
             dst_ref=kv_all.at[me, half, pl.ds(LANES * (1 - stage), LANES)],
-            send_sem=kv_send.at[head, half, stage], recv_sem=kv_recv.at[me, half],
+            send_sem=kv_send,
+            recv_sem=kv_recv.at[
+                jnp.where(jnp.logical_and(own, core == half), pair_at(me), me)
+            ],
             device_id=(sp, tp), device_id_type=MESH,
         )
 
@@ -149,14 +156,14 @@
         peer = lax.rem(z + (1 if way == 0 else NZ - 1), NZ) * NY + y
         return pltpu.make_async_remote_copy(
             src_ref=kv_all.at[block, core], dst_ref=kv_all.at[block, core],
-            send_sem=ring_send.at[block, way], recv_sem=kv_recv.at[block, core],
+            send_sem=ring_send.at[way], recv_sem=kv_recv.at[block],
             device_id=(peer, col), device_id_type=MESH,
         )
 
     def share_copy(block):
         return pltpu.make_async_remote_copy(
             src_ref=kv_all.at[block, core], dst_ref=kv_all.at[block, core],
-            send_sem=share_send.at[block], recv_sem=kv_recv.at[block, core],
+            send_sem=share_send, recv_sem=kv_recv.at[pair_at(block)],
             device_id=(me, sibling), device_id_type=MESH,
         )
 
@@ -167,7 +174,7 @@
         to_z, to_core = step // 2, lax.rem(step, 2)
         return pltpu.make_async_remote_copy(
             src_ref=q_own.at[head, rows_of(to_z, to_core, me)], dst_ref=q_all.at[me],
-            send_sem=q_send.at[head, step], recv_sem=q_recv.at[me],
+            send_sem=q_send, recv_sem=q_recv,
             device_id=(to_z * NY + core * 2 + head, place * 2 + to_core), device_id_type=MESH,
         )
 
@@ -186,7 +193,7 @@
     def back_copy(block):
         return pltpu.make_async_remote_copy(
             src_ref=packed.at[block], dst_ref=att.at[my_slot],
-            send_sem=back_send.at[block], recv_sem=back_recv.at[my_slot],
+            send_sem=back_send, recv_sem=back_recv,
             device_id=(block, back_owner(block)), device_id_type=MESH,
         )
 
@@ -225,11 +232,7 @@
         relay(token_copy, tok, tok_recv, turned[stage + 2], 1)
         for part in parts:
             relay(token_copy, tok, tok_recv, part, 2)
-        for part in parts:
-            arrived(tok.at[sibling, part], tok_recv.at[sibling, part])
-            for k in range(1, places):
-                block = lax.rem(place + k, places) * 2 + 1 - core
-                arrived(tok.at[block, part], tok_recv.at[block, part])
+        arrived(tok.at[pl.ds(0, 2)], tok_pair.at[stage])
         depth, model = tok.shape[2:]
         x = jnp.concatenate([tok[:, part].reshape(n_tp * depth, model) for part in parts], axis=0)
         both = jnp.dot(x, wqkv[...], preferred_element_type=F32)
@@ -263,9 +266,9 @@
         for head in range(2):
             kv_copy(head, 1, stage).start()
 
-    for part in range(PARTS):
+    for part in range(2):
         for kind in (1, 3, 0):
-            wo_copy(kind, turned[part] if kind == 3 else part).start()
+            wo_copy(kind, 1 - part if kind == 3 else part).start()
 
     for head in range(2):
 
@@ -274,12 +277,15 @@
             kv_all[me] = kv_own[head]
             q_all[me] = q_own[head, rows_of(z, core, me)]
 
-    for part in range(NY):
-        block = z * NY + part
-
-        @pl.when(jnp.logical_not(jnp.logical_and(block == me, mine)))
+    def halves_here(block):
+        return jnp.logical_and(block == me, mine)
+
+    for step in range(NY):
+        block = z * NY + lax.rem(y + step, NY)
+
+        @pl.when(jnp.logical_not(halves_here(block)))
         def _():
-            arrived(kv_all.at[block, core], kv_recv.at[block, core])
+            arrived(kv_all.at[block, core], kv_recv.at[block])
 
         for way in range(2):
             ring_copy(block, way).start()
@@ -288,16 +294,16 @@
         def _():
             share_copy(block).start()
 
-    def take_q(block, carry):
-        @pl.when(jnp.logical_not(jnp.logical_and(block == me, mine)))
-        def _():
-            arrived(q_all.at[block], q_recv.at[block])
-
-        return carry
-
-    lax.fori_loop(0, n_sp, take_q, 0)
-
-    def build(tile, carry):
+    def whole(count, less, buffer, sem):
+        for short in range(2):
+
+            @pl.when(less == (short == 1))
+            def _():
+                arrived(buffer.at[pl.ds(0, count - short)], sem)
+
+    whole(n_sp, mine, q_all, q_recv)
+
+    for tile in range(TILES):
         pieces = []
         for part in range(NY):
             pair = q_all[tile * NY + part].astype(F32)
@@ -306,9 +312,7 @@
         flipped = jnp.concatenate(pieces, axis=0).T
         q_top[tile] = flipped.astype(BF16)
         q_low[tile] = jnp.concatenate([flipped[DIM:], flipped[:DIM]], axis=0).astype(BF16)
-        return carry
-
-    lax.fori_loop(0, TILES, build, 0)
+
     arrived(bias_all.at[1 - core], bias_recv)
 
     def suffix(keep):
@@ -381,7 +385,7 @@
             seg_acc[group, tile + n] = acc[n]
             seg_keep[group, tile + n] = jnp.broadcast_to(keep[n], (8, LANES))
 
-    def attend(group, part):
+    def attend(group, part, between):
         count = TILES - group
         odd = lax.rem(count, 2)
         pairs = (count - 1) // 2
@@ -395,6 +399,8 @@
                     cover(group, part, group, 2 - single, True, 0)
                     if more:
                         cover(group, part, first, 2, False, 1)
+
+        between()
 
         @pl.when(pairs == 2)
         def _():
@@ -413,57 +419,65 @@
         behind = jnp.logical_or(jnp.logical_and(far, turn_of == 0), lax.rem(step, 2) == 0)
         part = jnp.where(jnp.logical_or(own, far), lax.rem(step, 2), turn_of // 2) * BATCH
         group = lax.rem(z + NZ + jnp.where(behind, -distance, distance), NZ)
-        return distance, behind, group, part
+        return group, part
+
+    def forward(index):
+        distance, turn_of = index // NZ + 1, lax.rem(index, NZ)
+        last = distance == NZ // 2
+        behind = lax.rem(index, 2) == 0
+        part = jnp.where(last, lax.rem(index, 2) * BATCH, 0) + turn_of // 2
+        group = lax.rem(z + NZ + jnp.where(behind, -distance, distance), NZ)
+        block = group * NY + part
+        arrived(kv_all.at[block, core], kv_recv.at[block])
+        for way in range(2):
+            onward = jnp.logical_or(
+                distance < 3, jnp.logical_and(distance == 3, (part < BATCH) == (way == 0))
+            )
+
+            @pl.when(jnp.logical_and(behind == (way == 0), onward))
+            def _():
+                ring_copy(block, way).start()
+
+        share_copy(block).start()
 
     def visit(step, carry):
-        ahead = step + 1
-
-        @pl.when(jnp.logical_and(ahead >= 2, ahead < STEPS))
-        def _():
-            distance, behind, group, part = stop_at(ahead)
-            for index in range(BATCH):
-                block = group * NY + part + index
-                arrived(kv_all.at[block, core], kv_recv.at[block, core])
-
-                @pl.when(
-                    jnp.logical_and(
-                        behind, jnp.logical_or(distance < 3, jnp.logical_and(distance == 3, part == 0))
-                    )
-                )
-                def _():
-                    ring_copy(block, 0).start()
-
-                @pl.when(
-                    jnp.logical_and(
-                        jnp.logical_not(behind),
-                        jnp.logical_or(distance < 3, jnp.logical_and(distance == 3, part > 0)),
-                    )
-                )
-                def _():
-                    ring_copy(block, 1).start()
-
-                share_copy(block).start()
+        def forward_if(low, high, index):
+            @pl.when(jnp.logical_and(step >= low, step < high))
+            def _():
+                forward(index)
+
+        forward_if(1, 2, 0)
+        forward_if(1, 2, 1)
+        forward_if(2, STEPS - 2, 2 * step)
 
         @pl.when(step == STEPS // 2)
         def _():
-            for part in range(PARTS):
+            for part in range(2):
                 relay(wo_copy, wfull, wo_recv, part, 3)
-                relay(wo_copy, wfull, wo_recv, turned[part], 1)
+                relay(wo_copy, wfull, wo_recv, 1 - part, 1)
 
         @pl.when(step == STEPS - 2)
         def _():
-            for part in range(PARTS):
+            for part in range(2):
                 relay(wo_copy, wfull, wo_recv, part, 2)
 
-        distance, behind, group, part = stop_at(step)
-        for index in range(BATCH):
-            block = group * NY + part + index
-
-            @pl.when(jnp.logical_not(jnp.logical_and(block == me, mine)))
+        group, part = stop_at(step)
+        block = group * NY + part
+        here = jnp.logical_and(block // BATCH == me // BATCH, mine)
+        for short in range(2):
+
+            @pl.when(here == (short == 1))
             def _():
-                arrived(kv_all.at[block, 1 - core], kv_recv.at[block, 1 - core])
-
-        attend(group, part)
+                arrived(
+                    kv_all.at[pl.ds(block, BATCH - short), 1 - core], kv_recv.at[pair_at(block)]
+                )
+
+        def between():
+            forward_if(1, 2, 2)
+            forward_if(1, 2, 3)
+            forward_if(2, STEPS - 2, 2 * step + 1)
+
+        attend(group, part, between)
         return carry
 
     lax.fori_loop(0, STEPS, visit, 0)
@@ -474,7 +488,7 @@
             acc = acc * seg_keep[group, tile][0:1] + seg_acc[group, tile]
         return acc
 
-    def deliver(pair, carry):
+    for pair in range(TILES // 2):
         flipped = jnp.concatenate([combine(2 * pair), combine(2 * pair + 1)], axis=0).T
         for part in range(NY):
             upper = flipped[SHARE * part : SHARE * part + 16]
@@ -492,75 +506,22 @@
                 def _():
                     back_copy(block).start()
 
-        return carry
-
-    lax.fori_loop(0, TILES // 2, deliver, 0)
-
     bias_copy.wait_send()
-    for part in range(PARTS):
-        for kind in range(2 * places - 1):
-            wo_copy(kind, part).wait_send()
-            token_copy(kind, part).wait_send()
-    for head in range(2):
-        for half in range(2):
-            for stage in range(2):
-                kv_copy(head, half, stage).wait_send()
-
-    def drain_q(step, carry):
-        for head in range(2):
-
-            @pl.when(jnp.logical_not(q_here(head, step)))
-            def _():
-                q_copy(head, step).wait_send()
-
-        return carry
-
-    lax.fori_loop(0, 2 * NZ, drain_q, 0)
-
-    def drain(block, carry):
-        ahead = lax.rem(z - block // NY + NZ, NZ)
-        behind = lax.rem(NZ - ahead, NZ)
-        first = lax.rem(block, NY) < NY // 2
-
-        @pl.when(jnp.logical_or(ahead < 3, jnp.logical_and(ahead == 3, first)))
-        def _():
-            ring_copy(block, 0).wait_send()
-
-        @pl.when(
-            jnp.logical_or(behind < 3, jnp.logical_and(behind == 3, jnp.logical_not(first)))
-        )
-        def _():
-            ring_copy(block, 1).wait_send()
-
-        @pl.when(block != me)
-        def _():
-            share_copy(block).wait_send()
-
-        return carry
-
-    lax.fori_loop(0, n_sp, drain, 0)
-
-    def drain_back(block, carry):
-        @pl.when(jnp.logical_not(back_here(block)))
-        def _():
-            back_copy(block).wait_send()
-
-        return carry
-
-    lax.fori_loop(0, n_sp, drain_back, 0)
-
-    source_z = lax.rem(col + n_sp - me, NZ)
+    arrived(wfull.at[pl.ds(0, n_tp - 1)], wo_send)
+    arrived(tok.at[pl.ds(0, n_tp - 1)], tok_send)
+    arrived(kv_own, kv_send)
+    whole(n_sp, mine, q_all, q_send)
+    for way in range(2):
+        arrived(kv_all.at[pl.ds(0, 14), 0], ring_send.at[way])
+    arrived(kv_all.at[pl.ds(0, n_sp - 1), 0], share_send)
+    whole(n_sp, back_here(me), att, back_send)
+    whole(n_sp, back_here(me), att, back_recv)
+
     for pair in range(n_tp):
         for sub in range(2):
             values = []
             for head in (2 * pair, 2 * pair + 1):
                 slot = head * 2 + sub
-                here = jnp.logical_and(source_z * NY + head % NY == me, 2 * (head // NY) + sub == col)
-
-                @pl.when(jnp.logical_not(here))
-                def _():
-                    arrived(att.at[slot], back_recv.at[slot])
-
                 values.append(att[slot].astype(F32))
             top = jnp.where(lane16 < DIM, values[0], turn(values[1]))
             low = jnp.where(lane16 < DIM, turn(values[0]), values[1])
@@ -568,16 +529,13 @@
             att_rows[SHARE * sub : SHARE * sub + 16, cols] = top.astype(BF16)
             att_rows[SHARE * sub + 16 : SHARE * (sub + 1), cols] = low.astype(BF16)
 
-    for part in range(PARTS):
-        arrived(wfull.at[sibling, part], wo_recv.at[sibling, part])
-        for k in range(1, places):
-            block = lax.rem(place + k, places) * 2 + 1 - core
-            arrived(wfull.at[block, part], wo_recv.at[block, part])
+    for part in range(2):
+        arrived(wfull.at[pl.ds(0, 2)], wo_pair.at[part])
 
     def put(first):
         return pltpu.make_async_copy(
             mixed.at[:, pl.ds(first, COLS)], out_ref.at[:, pl.ds(first, COLS)],
-            out_sem.at[first // COLS],
+            out_sem,
         )
 
     for first in range(0, out_ref.shape[1], COLS):
@@ -586,8 +544,7 @@
             att_rows[...], w, preferred_element_type=F32
         ).astype(BF16)
         put(first).start()
-    for first in range(0, out_ref.shape[1], COLS):
-        put(first).wait()
+    pltpu.make_async_copy(mixed, out_ref, out_sem).wait()
 
 
 def shards(tokens, w_query, w_key, w_value, head_bias, w_out):
@@ -596,7 +553,6 @@
     n_sp = lax.axis_size("sp")
     device_rows = tokens.shape[0]
     out_width = w_out.shape[1]
-    kinds = n_tp - 1
 
     smem = pl.BlockSpec(memory_space=pltpu.SMEM)
     anywhere = pl.BlockSpec(memory_space=pl.ANY)
@@ -613,7 +569,7 @@
         scratch_shapes=[
             vmem(n_tp, PARTS, device_rows // PARTS, model),
             vmem(model, 3 * local_width),
-            vmem(n_tp, PARTS, local_width // PARTS, out_width),
+            vmem(n_tp, 2, local_width // 2, out_width),
             pltpu.VMEM((n_tp, device_rows, 3 * local_width), F32),
             pltpu.VMEM((2, 2, 8, LANES), F32),
             vmem(2, 2, HALF, LANES),
@@ -631,22 +587,24 @@
             vmem(device_rows, n_tp * local_width),
             vmem(device_rows, out_width),
             pltpu.SemaphoreType.REGULAR,
-            dma((out_width // COLS,)),
+            dma,
             dma((5,)),
-            dma((kinds, PARTS)),
-            dma((n_tp, PARTS)),
-            dma((kinds, PARTS)),
-            dma((n_tp, PARTS)),
-            dma,
-            dma,
-            dma((2, 2, 2)),
-            dma((n_sp, 2)),
-            dma((n_sp, 2)),
-            dma((n_sp,)),
-            dma((2, 2 * NZ)),
-            dma((n_sp,)),
-            dma((n_sp,)),
-            dma((32,)),
+            dma,
+            dma((n_tp // 2, PARTS)),
+            dma((2,)),
+            dma,
+            dma((n_tp // 2, 2)),
+            dma((2,)),
+            dma,
+            dma,
+            dma,
+            dma((n_sp + n_sp // BATCH,)),
+            dma((2,)),
+            dma,
+            dma,
+            dma,
+            dma,
+            dma,
         ],
         compiler_params=pltpu.CompilerParams(
             collective_id=0, has_side_effects=True, vmem_limit_bytes=60 * 2**20
@@ -656,7 +614,7 @@
         head_bias,
         tokens.reshape(PARTS, device_rows // PARTS, model),
         w_query, w_key, w_value,
-        w_out.reshape(PARTS, local_width // PARTS, out_width),
+        w_out.reshape(2, local_width // 2, out_width),
     )
 
 

time: 75.3 us -> 73 us (0.969)
  Pallas kernels: 73 us -> 71.2 us
    pallas_call x1, Pallas kernels: 73 us -> 71.2 us  [shards(): pl.pallas_call(layer_kernel, out_shape=jax.ShapeDtypeStruct((device_rows,...]
where the time goes in v4:
time: 73 us; the launch traced here: 72.9 us
  Pallas kernels  71.2 us (98%)
  local copies, waits for them, and re-layouts  1.67 us (2%)
    pallas_call x1, Pallas kernels, shards(): pl.pallas_call(layer_kernel, out_shape=jax.ShapeDtypeStruct((device_rows,...  71.2 us
    unnamed x1, local copies, waits for them, and re-layouts  1.67 us

profile of v4, /device:TPU:25, one launch (start us, length us, event | category | flops | bytes accessed | tf_op | source)
XLA Modules:
  0.0 72.9 jit_solution(7617412547962257056)
XLA Ops:
  0.0 71.2 %layer.1 = bf16[64,2048]{1,0:T(8,128)(2,1)} custom-call(f32[2]{0:T(128)} %bias_ref.1, bf16[4,16,2048]{2,1,0:T(8,128)(2,1)} %bitcast.3, bf16[2048,128]{1,0:T(8,128)(2,1)} %wq_ref.1, bf16[2048,128]{1,0:T(8,128)(2,1)} %wk_ref.1, bf16[2048,128]{1,0:T(8,128)(2,1)} %wv_ref.1, bf16[2,64,2048]{2,1,0:T(8,128)(2,1)} %bitcast.2), custom_call_target="tpu_custom_call" | custom-call | tf_op jit(solution)/shard_map/layer/pallas_call | solution.py:564
  71.2 1.7 %copy.8 = bf16[64,2048]{1,0:T(8,128)(2,1)} copy(bf16[64,2048]{1,0:T(8,128)(2,1)} %layer.1) | data formatting | bytes 524288

commit v5 on v4

--- a/solution.py
+++ b/solution.py
@@ -21,10 +21,8 @@
 LANES = 128
 DIM = 64
 RUN = 64
-SHARE = 32
-SHARES = SEG // SHARE
-TILES = 8
-FAR = 1 << 20
+UNITS = 8
+SIDE = 4
 BATCH = 2
 STEPS = NZ * NY // BATCH
 
@@ -167,34 +165,57 @@
             device_id=(me, sibling), device_id_type=MESH,
         )
 
-    def rows_of(to_z, to_core, block):
-        return lax.rem(2 * to_z + to_core + 2 * block, SHARES)
+    def keeper(tile, chosen):
+        low = jnp.minimum(tile, NZ - 1 - tile)
+        return jnp.where(
+            low == 2, 3 * chosen, jnp.where(low == 3, 1, 4 + 2 * low) + chosen
+        )
+
+    low_tile = jnp.where(z >= 4, z // 2 - 2, jnp.where(lax.rem(z, 3) == 0, 2, 3))
+    chosen = jnp.where(z >= 4, lax.rem(z, 2), z // 2)
+
+    def rows_of(of_chosen, of_core, block):
+        return lax.rem(2 * of_chosen + of_core + block, SIDE)
+
+    def unit_block(unit):
+        tile = jnp.where(unit >= SIDE, NZ - 1 - low_tile, low_tile)
+        return tile * NY + lax.rem(unit, SIDE)
 
     def q_copy(head, step):
-        to_z, to_core = step // 2, lax.rem(step, 2)
+        to_chosen, to_core = step // 2, step % 2
+        unit = jnp.where(z >= NZ // 2, SIDE, 0) + y
         return pltpu.make_async_remote_copy(
-            src_ref=q_own.at[head, rows_of(to_z, to_core, me)], dst_ref=q_all.at[me],
+            src_ref=q_own.at[head, rows_of(to_chosen, to_core, me)], dst_ref=q_all.at[unit],
             send_sem=q_send, recv_sem=q_recv,
-            device_id=(to_z * NY + core * 2 + head, place * 2 + to_core), device_id_type=MESH,
+            device_id=(
+                keeper(z, to_chosen) * NY + core * 2 + head, place * 2 + to_core
+            ), device_id_type=MESH,
         )
 
     def q_here(head, step):
-        to_z, to_core = step // 2, lax.rem(step, 2)
-        return jnp.logical_and(to_z * NY + core * 2 + head == me, to_core == core)
-
-    def back_owner(block):
-        return lax.rem(z + block, n_tp)
-
-    my_slot = (place * NY + y) * 2 + core
-
-    def back_here(block):
-        return jnp.logical_and(block == me, back_owner(block) == col)
-
-    def back_copy(block):
+        to_chosen, to_core = step // 2, step % 2
+        return jnp.logical_and(
+            keeper(z, to_chosen) * NY + core * 2 + head == me, core == to_core
+        )
+
+    q_stays = jnp.logical_and(mine, jnp.logical_or(keeper(z, 0) == z, keeper(z, 1) == z))
+    my_slot = place * NY + y
+
+    def back_owner(unit, part):
+        return rows_of(chosen, core, unit_block(unit)) * 2 + part
+
+    def back_here(unit, part):
+        return jnp.logical_and(unit_block(unit) == me, back_owner(unit, part) == col)
+
+    back_stays = jnp.logical_and(
+        jnp.logical_or(low_tile == z, NZ - 1 - low_tile == z), rows_of(chosen, core, me) == place
+    )
+
+    def back_copy(unit, part):
         return pltpu.make_async_remote_copy(
-            src_ref=packed.at[block], dst_ref=att.at[my_slot],
+            src_ref=packed.at[unit, part], dst_ref=att.at[my_slot],
             send_sem=back_send, recv_sem=back_recv,
-            device_id=(block, back_owner(block)), device_id_type=MESH,
+            device_id=(unit_block(unit), back_owner(unit, part)), device_id_type=MESH,
         )
 
     for copy in loads:
@@ -202,24 +223,14 @@
     def turn(value):
         return pltpu.roll(value, DIM, 1)
 
-    lane16 = lax.broadcasted_iota(jnp.int32, (16, LANES), 1)
-
     def weave(upper, lower):
-        first = jnp.where(lane16 < DIM, upper, turn(lower)).astype(BF16)
-        second = jnp.where(lane16 < DIM, turn(upper), lower).astype(BF16)
+        left = lax.broadcasted_iota(jnp.int32, upper.shape, 1) < DIM
+        first = jnp.where(left, upper, turn(lower)).astype(BF16)
+        second = jnp.where(left, turn(upper), lower).astype(BF16)
         return first, second
 
     def strided(i, kind):
         return proj[:, RUN - 1 - i, kind * LANES : (kind + 1) * LANES]
-
-    def send_q(step, carry):
-        for head in range(2):
-
-            @pl.when(jnp.logical_not(q_here(head, step)))
-            def _():
-                q_copy(head, step).start()
-
-        return carry
 
     for part in range(PARTS // 2):
         relay(token_copy, tok, tok_recv, part, 3)
@@ -241,12 +252,25 @@
                 index * n_tp * depth : (index + 1) * n_tp * depth
             ].reshape(n_tp, depth, 3 * LANES)
         if stage == 1:
-            for share in range(SHARES):
-                block, first = share // 2, 32 * (share % 2)
-                q = proj[block, first : first + 32, 0:LANES] * (LOG2E * DIM ** (-0.5))
-                q_own[0, share], q_own[1, share] = weave(q[:16], q[16:])
+            for share in range(SIDE):
+                upper = proj[2 * share, :, 0:LANES] * (LOG2E * DIM ** (-0.5))
+                lower = proj[2 * share + 1, :, 0:LANES] * (LOG2E * DIM ** (-0.5))
+                q_own[0, share], q_own[1, share] = weave(upper, lower)
             pl.semaphore_wait(plane_sem, NZ - 1)
-            lax.fori_loop(0, 2 * NZ, send_q, 0)
+            for head in range(2):
+                for step in range(4):
+                    here = q_here(head, step)
+
+                    @pl.when(jnp.logical_not(here))
+                    def _():
+                        q_copy(head, step).start()
+
+                    @pl.when(here)
+                    def _():
+                        q_all[jnp.where(z >= NZ // 2, SIDE, 0) + y] = q_own[
+                            head, rows_of(step // 2, step % 2, me)
+                        ]
+
         base = 16 * (1 - stage)
         for i in range(base, base + 16, 2):
             upper = jnp.concatenate([strided(i, 1), strided(i + 1, 1)], axis=0)
@@ -275,7 +299,6 @@
         @pl.when(core * 2 + head == y)
         def _():
             kv_all[me] = kv_own[head]
-            q_all[me] = q_own[head, rows_of(z, core, me)]
 
     def halves_here(block):
         return jnp.logical_and(block == me, mine)
@@ -301,17 +324,15 @@
             def _():
                 arrived(buffer.at[pl.ds(0, count - short)], sem)
 
-    whole(n_sp, mine, q_all, q_recv)
-
-    for tile in range(TILES):
-        pieces = []
-        for part in range(NY):
-            pair = q_all[tile * NY + part].astype(F32)
-            pieces.append(jnp.where(lane16 < DIM, pair, 0.0))
-            pieces.append(jnp.where(lane16 < DIM, turn(pair), 0.0))
-        flipped = jnp.concatenate(pieces, axis=0).T
-        q_top[tile] = flipped.astype(BF16)
-        q_low[tile] = jnp.concatenate([flipped[DIM:], flipped[:DIM]], axis=0).astype(BF16)
+    whole(UNITS, q_stays, q_all, q_recv)
+
+    for unit in range(UNITS):
+        pair = q_all[unit].astype(F32)
+        left = lax.broadcasted_iota(jnp.int32, pair.shape, 1) < DIM
+        rows = [jnp.where(left, pair, 0.0), jnp.where(left, turn(pair), 0.0)]
+        flipped = jnp.concatenate(rows, axis=0).T
+        q_top[unit] = flipped.astype(BF16)
+        q_low[unit] = jnp.concatenate([flipped[DIM:], flipped[:DIM]], axis=0).astype(BF16)
 
     arrived(bias_all.at[1 - core], bias_recv)
 
@@ -349,10 +370,11 @@
             out = term if out is None else out + term
         return out, whole
 
-    def cover(group, part, tile, count, diagonal, bank):
+    def cover(group, part, unit, diagonal, bank):
+        count = 2
         width = count * LANES
         q = jnp.concatenate(
-            [q_top[tile + n] for n in range(count)] + [q_low[tile + n] for n in range(count)],
+            [q_top[unit + n] for n in range(count)] + [q_low[unit + n] for n in range(count)],
             axis=1,
         )
         bias = bias_all[head_core, head_local]
@@ -360,20 +382,18 @@
         if diagonal:
             lane = lax.broadcasted_iota(jnp.int32, (8, 2 * width), 1)
             row = lax.broadcasted_iota(jnp.int32, (8, 2 * width), 0)
-            half = lane // width
-            inside = lax.rem(lane, width)
-            owner = lax.rem(inside // SHARE, NY)
-            share = rows_of(z, core, tile * NY + owner)
-            query = SEG * owner + SHARE * share + lax.rem(inside, SHARE)
-            query = jnp.where(inside < LANES, query, FAR)
-            reach = query - row * RUN - (RUN - 1) + half * (RUN // 2) - SEG * part
+            half, inside = lane // width, lax.rem(lane, width)
+            owner = inside // LANES
+            share = rows_of(chosen, core, group * NY + part + owner)
+            query = SEG * owner + LANES * share + lax.rem(inside, LANES)
+            reach = query - row * RUN - (RUN - 1) + half * (RUN // 2)
         first = group * NY + part
         raw[bank, :, :, 0 : 2 * width] = jnp.dot(
             kv_all[pl.ds(first, BATCH), 0].reshape(BATCH * HALF, LANES), q,
             preferred_element_type=F32,
         ).reshape(BATCH, HALF, 2 * width)
-        acc = [seg_acc[group, tile + n] for n in range(count)]
-        keep = [seg_keep[group, tile + n][0:1] for n in range(count)]
+        acc = [seg_acc[group, unit + n] for n in range(count)]
+        keep = [seg_keep[group, unit + n][0:1] for n in range(count)]
         for index in range(BATCH):
             limit = reach - SEG * index if diagonal else None
             out, whole = segment(first + index, bank, index, width, bias, limit)
@@ -382,34 +402,35 @@
                 acc[n] = acc[n] * whole[:, lanes] + out[:, lanes]
                 keep[n] = keep[n] * whole[:, lanes]
         for n in range(count):
-            seg_acc[group, tile + n] = acc[n]
-            seg_keep[group, tile + n] = jnp.broadcast_to(keep[n], (8, LANES))
+            seg_acc[group, unit + n] = acc[n]
+            seg_keep[group, unit + n] = jnp.broadcast_to(keep[n], (8, LANES))
 
     def attend(group, part, between):
-        count = TILES - group
-        odd = lax.rem(count, 2)
-        pairs = (count - 1) // 2
-        first = group + 2 - odd
-
-        for single in range(2):
-            for more in range(2):
-
-                @pl.when(jnp.logical_and(odd == single, (pairs > 0) == (more == 1)))
-                def _():
-                    cover(group, part, group, 2 - single, True, 0)
-                    if more:
-                        cover(group, part, first, 2, False, 1)
-
-        between()
-
-        @pl.when(pairs == 2)
-        def _():
-            cover(group, part, first + 2, 2, False, 0)
-
-        @pl.when(pairs == 3)
-        def _():
-            cover(group, part, first + 2, 2, False, 0)
-            cover(group, part, first + 4, 2, False, 1)
+        def side(index, carry):
+            tile = jnp.where(index == 0, low_tile, NZ - 1 - low_tile)
+            base = index * SIDE
+
+            @pl.when(group < tile)
+            def _():
+                cover(group, part, base, False, 0)
+                cover(group, part, base + 2, False, 1)
+
+            @pl.when(jnp.logical_and(group == tile, part == 0))
+            def _():
+                cover(group, part, base, True, 0)
+                cover(group, part, base + 2, False, 1)
+
+            @pl.when(jnp.logical_and(group == tile, part > 0))
+            def _():
+                cover(group, part, base + 2, True, 0)
+
+            @pl.when(index == 0)
+            def _():
+                between()
+
+            return carry
+
+        lax.fori_loop(0, 2, side, 0)
 
     def stop_at(step):
         turn_of = lax.rem(step + 2, 4)
@@ -482,21 +503,21 @@
 
     lax.fori_loop(0, STEPS, visit, 0)
 
-    def combine(tile):
-        acc = seg_acc[0, tile]
+    def combine(unit):
+        acc = seg_acc[0, unit]
         for group in range(1, NZ):
-            acc = acc * seg_keep[group, tile][0:1] + seg_acc[group, tile]
+            acc = acc * seg_keep[group, unit][0:1] + seg_acc[group, unit]
         return acc
 
-    for pair in range(TILES // 2):
+    for pair in range(UNITS // 2):
         flipped = jnp.concatenate([combine(2 * pair), combine(2 * pair + 1)], axis=0).T
-        for part in range(NY):
-            upper = flipped[SHARE * part : SHARE * part + 16]
-            lower = flipped[SHARE * part + 16 : SHARE * (part + 1)]
+        for part in range(2):
+            upper = flipped[DIM * part : DIM * part + DIM // 2]
+            lower = flipped[DIM * part + DIM // 2 : DIM * (part + 1)]
             for n, folded in enumerate(weave(upper, lower)):
-                block = (2 * pair + n) * NY + part
-                packed[block] = folded
-                here = back_here(block)
+                unit = 2 * pair + n
+                packed[unit, part] = folded
+                here = back_here(unit, part)
 
                 @pl.when(here)
                 def _():
@@ -504,30 +525,23 @@
 
                 @pl.when(jnp.logical_not(here))
                 def _():
-                    back_copy(block).start()
+                    back_copy(unit, part).start()
 
     bias_copy.wait_send()
     arrived(wfull.at[pl.ds(0, n_tp - 1)], wo_send)
     arrived(tok.at[pl.ds(0, n_tp - 1)], tok_send)
     arrived(kv_own, kv_send)
-    whole(n_sp, mine, q_all, q_send)
+    whole(UNITS, q_stays, q_all, q_send)
     for way in range(2):
         arrived(kv_all.at[pl.ds(0, 14), 0], ring_send.at[way])
     arrived(kv_all.at[pl.ds(0, n_sp - 1), 0], share_send)
-    whole(n_sp, back_here(me), att, back_send)
-    whole(n_sp, back_here(me), att, back_recv)
+    whole(2 * UNITS, back_stays, att, back_send)
+    whole(2 * UNITS, back_stays, att, back_recv)
 
     for pair in range(n_tp):
-        for sub in range(2):
-            values = []
-            for head in (2 * pair, 2 * pair + 1):
-                slot = head * 2 + sub
-                values.append(att[slot].astype(F32))
-            top = jnp.where(lane16 < DIM, values[0], turn(values[1]))
-            low = jnp.where(lane16 < DIM, turn(values[0]), values[1])
-            cols = slice(pair * LANES, (pair + 1) * LANES)
-            att_rows[SHARE * sub : SHARE * sub + 16, cols] = top.astype(BF16)
-            att_rows[SHARE * sub + 16 : SHARE * (sub + 1), cols] = low.astype(BF16)
+        first, second = att[2 * pair].astype(F32), att[2 * pair + 1].astype(F32)
+        cols = slice(pair * LANES, (pair + 1) * LANES)
+        att_rows[0 : DIM // 2, cols], att_rows[DIM // 2 : DIM, cols] = weave(first, second)
 
     for part in range(2):
         arrived(wfull.at[pl.ds(0, 2)], wo_pair.at[part])
@@ -573,17 +587,17 @@
             pltpu.VMEM((n_tp, device_rows, 3 * local_width), F32),
             pltpu.VMEM((2, 2, 8, LANES), F32),
             vmem(2, 2, HALF, LANES),
-            vmem(2, SHARES, SHARE // 2, LANES),
-            vmem(n_sp, SHARE // 2, LANES),
+            vmem(2, SIDE, DIM, LANES),
+            vmem(UNITS, DIM, LANES),
             vmem(n_sp, 2, HALF, LANES),
-            vmem(TILES, LANES, LANES),
-            vmem(TILES, LANES, LANES),
+            vmem(UNITS, LANES, LANES),
+            vmem(UNITS, LANES, LANES),
             pltpu.VMEM((2, BATCH, HALF, 4 * LANES), F32),
             pltpu.VMEM((2, BATCH, HALF, 4 * LANES), F32),
-            pltpu.VMEM((NZ, TILES, DIM, LANES), F32),
-            pltpu.VMEM((NZ, TILES, 8, LANES), F32),
-            vmem(n_sp, SHARE // 2, LANES),
-            vmem(32, SHARE // 2, LANES),
+            pltpu.VMEM((NZ, UNITS, DIM, LANES), F32),
+            pltpu.VMEM((NZ, UNITS, 8, LANES), F32),
+            vmem(UNITS, 2, DIM // 2, LANES),
+            vmem(2 * UNITS, DIM // 2, LANES),
             vmem(device_rows, n_tp * local_width),
             vmem(device_rows, out_width),
             pltpu.SemaphoreType.REGULAR,

time: 73 us -> 75.5 us (1.034)
  the two profiles are of different devices: /device:TPU:25 before, /device:TPU:33 now
where the time goes in v5:
time: 75.5 us; the launch traced here: 75.3 us
  Pallas kernels  73.7 us (98%)
  local copies, waits for them, and re-layouts  1.67 us (2%)
    pallas_call x1, Pallas kernels, shards(): pl.pallas_call(layer_kernel, out_shape=jax.ShapeDtypeStruct((device_rows,...  73.7 us
    unnamed x1, local copies, waits for them, and re-layouts  1.67 us

profile of v5, /device:TPU:33, one launch (start us, length us, event | category | flops | bytes accessed | tf_op | source)
XLA Modules:
  0.0 75.3 jit_solution(7249077772923610638)
XLA Ops:
  0.0 73.7 %layer.1 = bf16[64,2048]{1,0:T(8,128)(2,1)} custom-call(f32[2]{0:T(128)} %bias_ref.1, bf16[4,16,2048]{2,1,0:T(8,128)(2,1)} %bitcast.3, bf16[2048,128]{1,0:T(8,128)(2,1)} %wq_ref.1, bf16[2048,128]{1,0:T(8,128)(2,1)} %wk_ref.1, bf16[2048,128]{1,0:T(8,128)(2,1)} %wv_ref.1, bf16[2,64,2048]{2,1,0:T(8,128)(2,1)} %bitcast.2), custom_call_target="tpu_custom_call" | custom-call | tf_op jit(solution)/shard_map/layer/pallas_call | solution.py:578
  73.7 1.7 %copy.8 = bf16[64,2048]{1,0:T(8,128)(2,1)} copy(bf16[64,2048]{1,0:T(8,128)(2,1)} %layer.1) | data formatting | bytes 524288

commit v6 on v5

--- a/solution.py
+++ b/solution.py
@@ -25,6 +25,8 @@
 SIDE = 4
 BATCH = 2
 STEPS = NZ * NY // BATCH
+INCOMING = (NZ - 1) * NY
+EASE = 3
 
 
 def layer_kernel(
@@ -167,12 +169,10 @@
 
     def keeper(tile, chosen):
         low = jnp.minimum(tile, NZ - 1 - tile)
-        return jnp.where(
-            low == 2, 3 * chosen, jnp.where(low == 3, 1, 4 + 2 * low) + chosen
-        )
-
-    low_tile = jnp.where(z >= 4, z // 2 - 2, jnp.where(lax.rem(z, 3) == 0, 2, 3))
-    chosen = jnp.where(z >= 4, lax.rem(z, 2), z // 2)
+        return lax.rem(2 * low + chosen + 5, NZ)
+
+    low_tile = lax.rem(z + 3, NZ) // 2
+    chosen = lax.rem(z + 3, 2)
 
     def rows_of(of_chosen, of_core, block):
         return lax.rem(2 * of_chosen + of_core + block, SIDE)
@@ -405,8 +405,9 @@
             seg_acc[group, unit + n] = acc[n]
             seg_keep[group, unit + n] = jnp.broadcast_to(keep[n], (8, LANES))
 
-    def attend(group, part, between):
-        def side(index, carry):
+    def attend(group, part, state):
+        def side(index, state):
+            passed, done = state
             tile = jnp.where(index == 0, low_tile, NZ - 1 - low_tile)
             base = index * SIDE
 
@@ -424,13 +425,12 @@
             def _():
                 cover(group, part, base + 2, True, 0)
 
-            @pl.when(index == 0)
-            def _():
-                between()
-
-            return carry
-
-        lax.fori_loop(0, 2, side, 0)
+            busy = jnp.where(group <= tile, 1, 0)
+            done = done + busy
+            more = jnp.where(done >= EASE, 2 * busy, 0)
+            return forward_to(passed, jnp.minimum(passed + more, INCOMING)), done
+
+        return lax.fori_loop(0, 2, side, state)
 
     def stop_at(step):
         turn_of = lax.rem(step + 2, 4)
@@ -461,15 +461,19 @@
 
         share_copy(block).start()
 
-    def visit(step, carry):
-        def forward_if(low, high, index):
-            @pl.when(jnp.logical_and(step >= low, step < high))
-            def _():
-                forward(index)
-
-        forward_if(1, 2, 0)
-        forward_if(1, 2, 1)
-        forward_if(2, STEPS - 2, 2 * step)
+    def forward_to(passed, target):
+        def one(index, carry):
+            forward(index)
+            return carry
+
+        target = jnp.maximum(passed, target)
+        lax.fori_loop(passed, target, one, 0)
+        return target
+
+    def visit(step, state):
+        passed, done = state
+        needed = jnp.where(step < 2, 0, 2 * step - 1 - lax.rem(step, 2))
+        passed = forward_to(passed, needed)
 
         @pl.when(step == STEPS // 2)
         def _():
@@ -493,15 +497,9 @@
                     kv_all.at[pl.ds(block, BATCH - short), 1 - core], kv_recv.at[pair_at(block)]
                 )
 
-        def between():
-            forward_if(1, 2, 2)
-            forward_if(1, 2, 3)
-            forward_if(2, STEPS - 2, 2 * step + 1)
-
-        attend(group, part, between)
-        return carry
-
-    lax.fori_loop(0, STEPS, visit, 0)
+        return attend(group, part, (passed, done))
+
+    lax.fori_loop(0, STEPS, visit, (jnp.int32(0), jnp.int32(0)))
 
     def combine(unit):
         acc = seg_acc[0, unit]

time: 75.5 us -> 76 us (level)
  the two profiles are of different devices: /device:TPU:33 before, /device:TPU:25 now
where the time goes in v6:
time: 76 us; the launch traced here: 75 us
  Pallas kernels  73.4 us (97%)
  local copies, waits for them, and re-layouts  1.67 us (2%)
    pallas_call x1, Pallas kernels, shards(): pl.pallas_call(layer_kernel, out_shape=jax.ShapeDtypeStruct((device_rows,...  73.4 us
    unnamed x1, local copies, waits for them, and re-layouts  1.67 us

profile of v6, /device:TPU:25, one launch (start us, length us, event | category | flops | bytes accessed | tf_op | source)
XLA Modules:
  0.0 75.0 jit_solution(10883544979950438100)
XLA Ops:
  0.0 73.4 %layer.1 = bf16[64,2048]{1,0:T(8,128)(2,1)} custom-call(f32[2]{0:T(128)} %bias_ref.1, bf16[4,16,2048]{2,1,0:T(8,128)(2,1)} %bitcast.3, bf16[2048,128]{1,0:T(8,128)(2,1)} %wq_ref.1, bf16[2048,128]{1,0:T(8,128)(2,1)} %wk_ref.1, bf16[2048,128]{1,0:T(8,128)(2,1)} %wv_ref.1, bf16[2,64,2048]{2,1,0:T(8,128)(2,1)} %bitcast.2), custom_call_target="tpu_custom_call" | custom-call | tf_op jit(solution)/shard_map/layer/pallas_call | solution.py:576
  73.4 1.7 %copy.8 = bf16[64,2048]{1,0:T(8,128)(2,1)} copy(bf16[64,2048]{1,0:T(8,128)(2,1)} %layer.1) | data formatting | bytes 524288

commit v7 on v4

--- a/solution.py
+++ b/solution.py
@@ -137,6 +137,18 @@
     def pair_at(block):
         return n_sp + block // BATCH
 
+    def early_at(part):
+        return n_sp + n_sp // BATCH + part
+
+    def own_copy(block, way, stage):
+        peer = lax.rem(z + (1 if way == 0 else NZ - 1), NZ) * NY + y
+        rows = pl.ds(LANES * (1 - stage), LANES)
+        return pltpu.make_async_remote_copy(
+            src_ref=kv_all.at[block, core, rows], dst_ref=kv_all.at[block, core, rows],
+            send_sem=ring_send.at[way], recv_sem=kv_recv.at[block],
+            device_id=(peer, col), device_id_type=MESH,
+        )
+
     def kv_copy(head, half, stage):
         aim = core * 2 + head
         own = aim == y
@@ -147,7 +159,11 @@
             dst_ref=kv_all.at[me, half, pl.ds(LANES * (1 - stage), LANES)],
             send_sem=kv_send,
             recv_sem=kv_recv.at[
-                jnp.where(jnp.logical_and(own, core == half), pair_at(me), me)
+                jnp.where(
+                    jnp.logical_and(own, core == half),
+                    pair_at(me),
+                    early_at(y) if stage == 0 else me,
+                )
             ],
             device_id=(sp, tp), device_id_type=MESH,
         )
@@ -280,19 +296,27 @@
     def halves_here(block):
         return jnp.logical_and(block == me, mine)
 
-    for step in range(NY):
-        block = z * NY + lax.rem(y + step, NY)
-
-        @pl.when(jnp.logical_not(halves_here(block)))
-        def _():
-            arrived(kv_all.at[block, core], kv_recv.at[block])
-
-        for way in range(2):
-            ring_copy(block, way).start()
-
-        @pl.when(block != me)
-        def _():
-            share_copy(block).start()
+    for stage in range(2):
+        for step in range(NY):
+            part = lax.rem(y + step, NY)
+            block = z * NY + part
+            rows = pl.ds(LANES * (1 - stage), LANES)
+
+            @pl.when(jnp.logical_not(halves_here(block)))
+            def _():
+                arrived(
+                    kv_all.at[block, core, rows],
+                    kv_recv.at[early_at(part) if stage == 0 else block],
+                )
+
+            for way in range(2):
+                own_copy(block, way, stage).start()
+
+            if stage == 1:
+
+                @pl.when(block != me)
+                def _():
+                    share_copy(block).start()
 
     def whole(count, less, buffer, sem):
         for short in range(2):
@@ -598,7 +622,7 @@
             dma,
             dma,
             dma,
-            dma((n_sp + n_sp // BATCH,)),
+            dma((n_sp + n_sp // BATCH + NY,)),
             dma((2,)),
             dma,
             dma,

time: 73 us -> 71.2 us (0.975)
  Pallas kernels: 71.2 us -> 69.3 us
    pallas_call x1, Pallas kernels: 71.2 us -> 69.3 us  [shards(): pl.pallas_call(layer_kernel, out_shape=jax.ShapeDtypeStruct((device_rows,...]
where the time goes in v7:
time: 71.2 us; the launch traced here: 71 us
  Pallas kernels  69.3 us (97%)
  local copies, waits for them, and re-layouts  1.67 us (2%)
    pallas_call x1, Pallas kernels, shards(): pl.pallas_call(layer_kernel, out_shape=jax.ShapeDtypeStruct((device_rows,...  69.3 us
    unnamed x1, local copies, waits for them, and re-layouts  1.67 us

profile of v7, /device:TPU:25, one launch (start us, length us, event | category | flops | bytes accessed | tf_op | source)
XLA Modules:
  0.0 71.0 jit_solution(9564293132936592140)
XLA Ops:
  0.0 69.3 %layer.1 = bf16[64,2048]{1,0:T(8,128)(2,1)} custom-call(f32[2]{0:T(128)} %bias_ref.1, bf16[4,16,2048]{2,1,0:T(8,128)(2,1)} %bitcast.3, bf16[2048,128]{1,0:T(8,128)(2,1)} %wq_ref.1, bf16[2048,128]{1,0:T(8,128)(2,1)} %wk_ref.1, bf16[2048,128]{1,0:T(8,128)(2,1)} %wv_ref.1, bf16[2,64,2048]{2,1,0:T(8,128)(2,1)} %bitcast.2), custom_call_target="tpu_custom_call" | custom-call | tf_op jit(solution)/shard_map/layer/pallas_call | solution.py:588
  69.3 1.7 %copy.8 = bf16[64,2048]{1,0:T(8,128)(2,1)} copy(bf16[64,2048]{1,0:T(8,128)(2,1)} %layer.1) | data formatting | bytes 524288

commit v8 on v7

--- a/solution.py
+++ b/solution.py
@@ -228,7 +228,8 @@
     def strided(i, kind):
         return proj[:, RUN - 1 - i, kind * LANES : (kind + 1) * LANES]
 
-    def send_q(step, carry):
+    def send_q(stage, to_z, carry):
+        step = 2 * to_z + stage
         for head in range(2):
 
             @pl.when(jnp.logical_not(q_here(head, step)))
@@ -256,13 +257,15 @@
             proj[:, part * depth : (part + 1) * depth, :] = both[
                 index * n_tp * depth : (index + 1) * n_tp * depth
             ].reshape(n_tp, depth, 3 * LANES)
-        if stage == 1:
-            for share in range(SHARES):
-                block, first = share // 2, 32 * (share % 2)
-                q = proj[block, first : first + 32, 0:LANES] * (LOG2E * DIM ** (-0.5))
-                q_own[0, share], q_own[1, share] = weave(q[:16], q[16:])
+        for block in range(n_tp):
+            scale = LOG2E * DIM ** (-0.5)
+            upper = proj[block, 16 * stage : 16 * stage + 16, 0:LANES] * scale
+            lower = proj[block, 16 * stage + 32 : 16 * stage + 48, 0:LANES] * scale
+            share = 2 * block + stage
+            q_own[0, share], q_own[1, share] = weave(upper, lower)
+        if stage == 0:
             pl.semaphore_wait(plane_sem, NZ - 1)
-            lax.fori_loop(0, 2 * NZ, send_q, 0)
+        lax.fori_loop(0, NZ, functools.partial(send_q, stage), 0)
         base = 16 * (1 - stage)
         for i in range(base, base + 16, 2):
             upper = jnp.concatenate([strided(i, 1), strided(i + 1, 1)], axis=0)
@@ -388,7 +391,8 @@
             inside = lax.rem(lane, width)
             owner = lax.rem(inside // SHARE, NY)
             share = rows_of(z, core, tile * NY + owner)
-            query = SEG * owner + SHARE * share + lax.rem(inside, SHARE)
+            place_in = 32 * (lax.rem(inside, SHARE) // 16) + lax.rem(inside, 16)
+            query = SEG * owner + 64 * (share // 2) + 16 * lax.rem(share, 2) + place_in
             query = jnp.where(inside < LANES, query, FAR)
             reach = query - row * RUN - (RUN - 1) + half * (RUN // 2) - SEG * part
         first = group * NY + part
@@ -470,9 +474,9 @@
             def _():
                 forward(index)
 
-        forward_if(1, 2, 0)
-        forward_if(1, 2, 1)
-        forward_if(2, STEPS - 2, 2 * step)
+        forward_if(2, 3, 2)
+        forward_if(2, 3, 3)
+        forward_if(3, STEPS - 2, 2 * step)
 
         @pl.when(step == STEPS // 2)
         def _():
@@ -497,8 +501,9 @@
                 )
 
         def between():
-            forward_if(1, 2, 2)
-            forward_if(1, 2, 3)
+            forward_if(1, 2, 0)
+            forward_if(1, 2, 1)
+            forward_if(2, 3, 4)
             forward_if(2, STEPS - 2, 2 * step + 1)
 
         attend(group, part, between)
@@ -550,8 +555,8 @@
             top = jnp.where(lane16 < DIM, values[0], turn(values[1]))
             low = jnp.where(lane16 < DIM, turn(values[0]), values[1])
             cols = slice(pair * LANES, (pair + 1) * LANES)
-            att_rows[SHARE * sub : SHARE * sub + 16, cols] = top.astype(BF16)
-            att_rows[SHARE * sub + 16 : SHARE * (sub + 1), cols] = low.astype(BF16)
+            att_rows[16 * sub : 16 * sub + 16, cols] = top.astype(BF16)
+            att_rows[16 * sub + 32 : 16 * sub + 48, cols] = low.astype(BF16)
 
     for part in range(2):
         arrived(wfull.at[pl.ds(0, 2)], wo_pair.at[part])

time: 71.2 us -> 71.1 us (level)
  no operation moved by 1% of the time
where the time goes in v8:
time: 71.1 us; the launch traced here: 70.3 us
  Pallas kernels  68.7 us (97%)
  local copies, waits for them, and re-layouts  1.67 us (2%)
    pallas_call x1, Pallas kernels, shards(): pl.pallas_call(layer_kernel, out_shape=jax.ShapeDtypeStruct((device_rows,...  68.7 us
    unnamed x1, local copies, waits for them, and re-layouts  1.67 us

profile of v8, /device:TPU:25, one launch (start us, length us, event | category | flops | bytes accessed | tf_op | source)
XLA Modules:
  0.0 70.3 jit_solution(4749919131678331756)
XLA Ops:
  0.0 68.7 %layer.1 = bf16[64,2048]{1,0:T(8,128)(2,1)} custom-call(f32[2]{0:T(128)} %bias_ref.1, bf16[4,16,2048]{2,1,0:T(8,128)(2,1)} %bitcast.3, bf16[2048,128]{1,0:T(8,128)(2,1)} %wq_ref.1, bf16[2048,128]{1,0:T(8,128)(2,1)} %wk_ref.1, bf16[2048,128]{1,0:T(8,128)(2,1)} %wv_ref.1, bf16[2,64,2048]{2,1,0:T(8,128)(2,1)} %bitcast.2), custom_call_target="tpu_custom_call" | custom-call | tf_op jit(solution)/shard_map/layer/pallas_call | solution.py:593
  68.7 1.7 %copy.8 = bf16[64,2048]{1,0:T(8,128)(2,1)} copy(bf16[64,2048]{1,0:T(8,128)(2,1)} %layer.1) | data formatting | bytes 524288

commit v9 on v8

--- a/solution.py
+++ b/solution.py
@@ -257,15 +257,6 @@
             proj[:, part * depth : (part + 1) * depth, :] = both[
                 index * n_tp * depth : (index + 1) * n_tp * depth
             ].reshape(n_tp, depth, 3 * LANES)
-        for block in range(n_tp):
-            scale = LOG2E * DIM ** (-0.5)
-            upper = proj[block, 16 * stage : 16 * stage + 16, 0:LANES] * scale
-            lower = proj[block, 16 * stage + 32 : 16 * stage + 48, 0:LANES] * scale
-            share = 2 * block + stage
-            q_own[0, share], q_own[1, share] = weave(upper, lower)
-        if stage == 0:
-            pl.semaphore_wait(plane_sem, NZ - 1)
-        lax.fori_loop(0, NZ, functools.partial(send_q, stage), 0)
         base = 16 * (1 - stage)
         for i in range(base, base + 16, 2):
             upper = jnp.concatenate([strided(i, 1), strided(i + 1, 1)], axis=0)
@@ -284,6 +275,15 @@
                 kv_own[head, 1, at : at + DIM] = flipped[DIM * head : DIM * (head + 1)]
         for head in range(2):
             kv_copy(head, 1, stage).start()
+        for block in range(n_tp):
+            scale = LOG2E * DIM ** (-0.5)
+            upper = proj[block, 16 * stage : 16 * stage + 16, 0:LANES] * scale
+            lower = proj[block, 16 * stage + 32 : 16 * stage + 48, 0:LANES] * scale
+            share = 2 * block + stage
+            q_own[0, share], q_own[1, share] = weave(upper, lower)
+        if stage == 0:
+            pl.semaphore_wait(plane_sem, NZ - 1)
+        lax.fori_loop(0, NZ, functools.partial(send_q, stage), 0)
 
     for part in range(2):
         for kind in (1, 3, 0):

time: 71.1 us -> 70.6 us (level)
  no operation moved by 1% of the time
where the time goes in v9:
time: 70.6 us; the launch traced here: 70.5 us
  Pallas kernels  68.8 us (97%)
  local copies, waits for them, and re-layouts  1.67 us (2%)
    pallas_call x1, Pallas kernels, shards(): pl.pallas_call(layer_kernel, out_shape=jax.ShapeDtypeStruct((device_rows,...  68.8 us
    unnamed x1, local copies, waits for them, and re-layouts  1.67 us

profile of v9, /device:TPU:25, one launch (start us, length us, event | category | flops | bytes accessed | tf_op | source)
XLA Modules:
  0.0 70.5 jit_solution(10412741475243029768)
XLA Ops:
  0.0 68.8 %layer.1 = bf16[64,2048]{1,0:T(8,128)(2,1)} custom-call(f32[2]{0:T(128)} %bias_ref.1, bf16[4,16,2048]{2,1,0:T(8,128)(2,1)} %bitcast.3, bf16[2048,128]{1,0:T(8,128)(2,1)} %wq_ref.1, bf16[2048,128]{1,0:T(8,128)(2,1)} %wk_ref.1, bf16[2048,128]{1,0:T(8,128)(2,1)} %wv_ref.1, bf16[2,64,2048]{2,1,0:T(8,128)(2,1)} %bitcast.2), custom_call_target="tpu_custom_call" | custom-call | tf_op jit(solution)/shard_map/layer/pallas_call | solution.py:593
  68.8 1.7 %copy.8 = bf16[64,2048]{1,0:T(8,128)(2,1)} copy(bf16[64,2048]{1,0:T(8,128)(2,1)} %layer.1) | data formatting | bytes 524288
